TPU v7x, 32 devices: a whole 2x2x4 slice. The times are simulated.
32 devices in a mesh: sp: 8 (over z, x), tp: 4 (over y, core).
Axes of the slice: x: 2, y: 2, z: 4, core: 2. Of those that a mesh axis runs over, the one named last changes fastest.
Arguments:
- cotangent: bfloat16 [2048, 2048], P('sp', 'tp'), may hold values from -6 to 6
- moe_input: bfloat16 [2048, 2048], P('sp', 'tp'), may hold values from -6 to 6
- routes: int32 [2048, 2], P('sp'), may hold values from 0 to 7, all different within a row; in each aligned block of 256 rows (0 to 255, 256 to 511, ...) at most 96 rows name the same one
- gates: float32 [2048, 2], P('sp'), may hold values from 0.1 to 1
- w_gate: bfloat16 [8, 2048, 2048], P('sp', None, 'tp'), may hold values from -0.125 to 0.125
- w_up: bfloat16 [8, 2048, 2048], P('sp', None, 'tp'), may hold values from -0.125 to 0.125
- w_down: bfloat16 [8, 2048, 2048], P('sp', 'tp'), may hold values from -0.125 to 0.125
- out_proj: bfloat16 [1024, 2048], P('tp'), may hold values from -0.1875 to 0.1875
- conv_in: bfloat16 [1024, 2048], P('tp', 'sp'), may hold values from -6 to 6
- branch: bfloat16 [1024, 2048], P('tp', 'sp'), may hold values from -6 to 6
- state_before: float32 [1024, 2048], P('tp', 'sp'), may hold values from -6 to 6
- state_after: float32 [1024, 2048], P('tp', 'sp'), may hold values from -6 to 6
- jump: float32 [1024, 2048], P('tp', 'sp'), may hold values from -2 to 0, as said below
- recur_weight: bfloat16 [2, 16, 64, 64], P(None, 'tp'), may hold values from -0.75 to 0.75
- input_weight: bfloat16 [2, 16, 64, 64], P(None, 'tp'), may hold values from -0.75 to 0.75
- lam: float32 [2, 1024], P(None, 'tp')
Outputs:
- gate_grad: bfloat16 [8, 2048, 2048], P('sp', None, 'tp')
- up_grad: bfloat16 [8, 2048, 2048], P('sp', None, 'tp')
- down_grad: bfloat16 [8, 2048, 2048], P('sp', 'tp')
- residual_grad: bfloat16 [2048, 2048], P('sp', 'tp')
- out_proj_grad: float32 [1024, 2048], P('tp', 'sp')
- conv_grad: float32 [1024, 2048], P('tp', 'sp')
- branch_grad: float32 [1024, 2048], P('tp', 'sp')
Inputs may be any that keep to these rules, and one draw needn't show every extreme that they name: `routes`: each token names 2 different experts. Among the tokens of one index of sp (aligned blocks of 256 rows) no expert is named more than 96 times, a bound that some block reaches. `jump`: every entry is at most -1 / 20480.
All inputs are finite; a program needn't handle non-finite values.
Results may differ from a plain program's by a relative error of at most 0.02.
Values may be sent and summed in bfloat16 or wider, within the bound.
No kernel may reach another device: no remote copies, remote signals or barrier semaphores. Data moves between devices by JAX's collectives and lax.ppermute only.
A program may use at most 128 MiB of HBM per device.

v0:
```python
import functools

import jax
import jax.numpy as jnp
from jax import lax
from jax.experimental import pallas as pl
from jax.experimental.pallas import tpu as pltpu
from jax.sharding import PartitionSpec as P


decay_scale = 8.0
f32 = jnp.float32
bf16 = jnp.bfloat16

nn = (((1,), (0,)), ((), ()))
nt = (((1,), (1,)), ((), ()))
tn = (((0,), (0,)), ((), ()))


def dot(a, b, dims):
    return lax.dot_general(a, b, dims, preferred_element_type=f32)


def call(kernel, inputs, outs, scratch=(), flops=0, scalars=1, grant=12, free=0):
    moved = sum(a.size * a.dtype.itemsize for a in inputs) + sum(
        o.size * o.dtype.itemsize for o in outs
    )
    specs = [pl.BlockSpec(memory_space=pltpu.SMEM)] * scalars
    specs += [pl.BlockSpec(memory_space=pl.ANY)] * free
    specs += [pl.BlockSpec(memory_space=pltpu.VMEM)] * (len(inputs) - scalars - free)
    return pl.pallas_call(
        kernel,
        out_shape=tuple(outs),
        in_specs=specs,
        out_specs=tuple(pl.BlockSpec(memory_space=pltpu.VMEM) for _ in outs),
        scratch_shapes=list(scratch),
        cost_estimate=pl.CostEstimate(
            flops=int(flops), bytes_accessed=int(moved), transcendentals=0
        ),
        compiler_params=pltpu.CompilerParams(vmem_limit_bytes=grant * 1024 * 1024),
    )(*inputs)


def shape(dims, kind):
    return jax.ShapeDtypeStruct(dims, kind)


def pack_kernel(experts, capacity, place_ref, *refs):
    far, out_refs, near, sems = refs[:4], refs[4 : 5 + experts], refs[5 + experts : -1], refs[-1]
    fetches = [
        pltpu.make_async_copy(a, b, sems.at[i]) for i, (a, b) in enumerate(zip(far, near))
    ]
    for fetch in fetches:
        fetch.start()
    routes_ref, gates_ref, rows_ref, cot_ref = near
    position_ref, blocks = out_refs[0], out_refs[1:]
    fetches[0].wait()
    fetches[1].wait()
    top, tokens = routes_ref.shape
    filler = jnp.zeros((8 - 2 * top % 8, tokens), f32)
    table = jnp.concatenate([routes_ref[...].astype(f32), gates_ref[...], filler], axis=0).T
    width = rows_ref.shape[1]
    lanes = max(128, experts)
    named = lax.broadcasted_iota(jnp.int32, (tokens, lanes), 1)
    picks = [table[:, k : k + 1].astype(jnp.int32) for k in range(top)]
    onehots = [(pick == named).astype(f32) for pick in picks]
    both = functools.reduce(jnp.add, onehots).astype(bf16)
    before = (
        lax.broadcasted_iota(jnp.int32, (tokens, tokens), 0)
        > lax.broadcasted_iota(jnp.int32, (tokens, tokens), 1)
    ).astype(f32).astype(bf16)
    earlier = dot(before, both, nn)
    positions = [
        jnp.sum(earlier * onehot, axis=1, keepdims=True).astype(jnp.int32) for onehot in onehots
    ]
    for k in range(top):
        position_ref[:, k : k + 1] = picks[k]
        position_ref[:, top + k : top + k + 1] = positions[k]
    for fetch in fetches[2:]:
        fetch.wait()
    rows = rows_ref[...]
    cot = cot_ref[...].astype(f32)
    scaled = [(cot * table[:, top + k : top + k + 1]).astype(bf16) for k in range(top)]
    slot = lax.broadcasted_iota(jnp.int32, (tokens, capacity), 1)
    for s in range(experts):
        expert = place_ref[0] ^ s
        selects = [
            (jnp.where(pick == expert, position, -1) == slot).astype(f32).astype(bf16)
            for pick, position in zip(picks, positions)
        ]
        blocks[s][:, :width] = dot(functools.reduce(jnp.add, selects), rows, tn).astype(bf16)
        grads = functools.reduce(jnp.add, [dot(sel, sc, tn) for sel, sc in zip(selects, scaled)])
        blocks[s][:, width:] = grads.astype(bf16)


def combine_kernel(experts, place_ref, table_ref, cot_ref, *refs):
    blocks, out_ref = refs[:experts], refs[experts]
    tokens, top = table_ref.shape[0], table_ref.shape[1] // 2
    capacity = blocks[0].shape[0]
    slot = lax.broadcasted_iota(jnp.int32, (tokens, capacity), 1)
    total = cot_ref[...].astype(f32)
    added = jnp.zeros_like(total)
    for s in range(experts):
        expert = place_ref[0] ^ s
        select = functools.reduce(
            jnp.add,
            [
                (
                    jnp.where(
                        table_ref[:, k : k + 1] == expert, table_ref[:, top + k : top + k + 1], -1
                    )
                    == slot
                ).astype(f32)
                for k in range(top)
            ],
        ).astype(bf16)
        added = added + dot(select, blocks[s][...], nn)
    out_ref[...] = (total + added).astype(bf16)


def bit_order(count):
    bits = count.bit_length() - 1
    return [int(format(i, "0%db" % bits)[::-1], 2) if bits else 0 for i in range(count)]


def expert_kernel(ranks, chunks, place_ref, *refs):
    parts = [refs[c * ranks : (c + 1) * ranks] for c in range(chunks)]
    gate_ref, up_ref, down_ref = refs[ranks * chunks : ranks * chunks + 3]
    keep_ref, send_ref, act_ref, gate_hid_ref, up_hid_ref = refs[ranks * chunks + 3 :]
    width = parts[0][0].shape[1] // 2
    hidden = gate_ref.shape[1]
    tile = min(256, hidden)
    place = place_ref[0]
    offsets = [pl.multiple_of((place ^ r) * width, width) for r in range(ranks)]
    for h in range(hidden // tile):
        cols = slice(h * tile, (h + 1) * tile)
        pre_gate = pre_up = act_grad = None
        for r in range(ranks):
            rows = jnp.concatenate([part[r][:, :width] for part in parts], axis=0)
            grads = jnp.concatenate([part[r][:, width:] for part in parts], axis=0)
            where = pl.ds(offsets[r], width)
            one = dot(rows, gate_ref[where, cols], nn)
            two = dot(rows, up_ref[where, cols], nn)
            three = dot(grads, down_ref[cols, where], nt)
            pre_gate = one if r == 0 else pre_gate + one
            pre_up = two if r == 0 else pre_up + two
            act_grad = three if r == 0 else act_grad + three
        sig = 1.0 / (1.0 + jnp.exp(-pre_gate))
        silu = pre_gate * sig
        slope = sig * (1.0 + pre_gate * (1.0 - sig))
        act_ref[:, cols] = (silu * pre_up).astype(bf16)
        up_hid_ref[:, cols] = (act_grad * silu).astype(bf16)
        gate_hid_ref[:, cols] = (act_grad * pre_up * slope).astype(bf16)
    gate_hid = gate_hid_ref[...]
    up_hid = up_hid_ref[...]
    half = ranks // 2
    order = bit_order(ranks)
    for i in [*range(half, ranks), *range(half)]:
        where = pl.ds(offsets[order[i]], width)
        part = dot(gate_hid, gate_ref[where, :], nt) + dot(up_hid, up_ref[where, :], nt)
        if i < half:
            keep_ref[i] = part.astype(bf16)
        else:
            send_ref[i - half] = part.astype(bf16)


def weight_kernel(ranks, chunks, groups, place_ref, *refs):
    parts = [refs[c * ranks : (c + 1) * ranks] for c in range(chunks)]
    rest = refs[chunks * ranks :]
    gate_hids, up_hids = rest[:groups], rest[groups : 2 * groups]
    gate_out, up_out, gate_buf, up_buf, sems = rest[2 * groups :]
    width = parts[0][0].shape[1] // 2
    gate_hid = jnp.concatenate([ref[...] for ref in gate_hids], axis=0)
    up_hid = jnp.concatenate([ref[...] for ref in up_hids], axis=0)
    copies = []
    for r in range(ranks):
        where = pl.ds(pl.multiple_of((place_ref[0] ^ r) * width, width), width)
        rows = jnp.concatenate([part[r][:, :width] for part in parts], axis=0).T
        for j, (hid, buf, out) in enumerate(
            ((gate_hid, gate_buf, gate_out), (up_hid, up_buf, up_out))
        ):
            buf[r] = dot(rows, hid, nn).astype(bf16)
            copies.append(pltpu.make_async_copy(buf.at[r], out.at[where, :], sems.at[j, r]))
            copies[-1].start()
    for copy in copies:
        copy.wait()


def down_kernel(ranks, chunks, groups, place_ref, *refs):
    parts = [refs[c * ranks : (c + 1) * ranks] for c in range(chunks)]
    hids = refs[chunks * ranks : chunks * ranks + groups]
    out, buf, sems = refs[chunks * ranks + groups :]
    width = parts[0][0].shape[1] // 2
    hid = jnp.concatenate([ref[...] for ref in hids], axis=0).T
    copies = []
    for r in range(ranks):
        where = pl.ds(pl.multiple_of((place_ref[0] ^ r) * width, width), width)
        grads = jnp.concatenate([part[r][:, width:] for part in parts], axis=0)
        buf[r] = dot(hid, grads, nn).astype(bf16)
        copies.append(pltpu.make_async_copy(buf.at[r], out.at[:, where], sems.at[r]))
        copies[-1].start()
    for copy in copies:
        copy.wait()


def ticket_kernel(place_ref, out_ref):
    out_ref[0] = place_ref[0]


def ticket(place, flops):
    return pl.pallas_call(
        ticket_kernel,
        out_shape=shape((1,), jnp.int32),
        in_specs=[pl.BlockSpec(memory_space=pltpu.SMEM)],
        out_specs=pl.BlockSpec(memory_space=pltpu.SMEM),
        cost_estimate=pl.CostEstimate(flops=int(flops), bytes_accessed=8, transcendentals=0),
        compiler_params=pltpu.CompilerParams(vmem_limit_bytes=1024 * 1024),
        name="ticket",
    )(place)


def shifted(values, step, reverse, fill):
    length = values.shape[1]
    lane = lax.broadcasted_iota(jnp.int32, values.shape, 1)
    if reverse:
        return jnp.where(lane < length - step, pltpu.roll(values, length - step, 1), fill)
    return jnp.where(lane >= step, pltpu.roll(values, step, 1), fill)


def one_less_exp(power, value):
    series = 1.0 + power * (1.0 / 7.0)
    for term in range(6, 1, -1):
        series = 1.0 + power * (1.0 / term) * series
    return jnp.where(power > -0.35, -power * series, 1.0 - value)


def softplus(value):
    small = jnp.exp(-jnp.abs(value))
    series = 1.0 / 7.0
    for term in range(6, 0, -1):
        series = 1.0 / term - small * series
    return jnp.maximum(value, 0.0) + jnp.where(small < 0.05, small * series, jnp.log(1.0 + small))


def sigmoid(value):
    return 1.0 / (1.0 + jnp.exp(-value))


def gates_kernel(
    recur_maps, input_maps, lam_ref, conv_ref, before_ref, after_ref, jump_ref, branch_ref,
    mix_ref, gelu_ref, back_ref, decay_ref, direct_ref, recur_ref, inward_ref,
):
    blocks, size = recur_maps.shape[1], recur_maps.shape[2]
    channels = blocks * size
    rates = decay_scale * softplus(-lam_ref[...])
    rates = jnp.concatenate([rates, jnp.zeros((6, channels), f32)], axis=0).T
    for b in range(blocks):
        part = slice(b * size, (b + 1) * size)
        conv_in = conv_ref[part, :]
        conv = conv_in.astype(f32)
        jump = jump_ref[part, :]
        lru = None
        for d, state_ref in enumerate((before_ref, after_ref)):
            state = state_ref[part, :]
            recur = sigmoid(dot(recur_maps[d, b], conv_in, tn))
            inward = sigmoid(dot(input_maps[d, b], conv_in, tn))
            speed = rates[part, d : d + 1]
            log_decay = jump - speed * recur
            decay = jnp.exp(log_decay)
            root = jnp.sqrt(one_less_exp(2.0 * log_decay, decay * decay))
            gated = inward * conv
            term = decay * state + root * gated
            lru = term if d == 0 else lru + term
            decay_ref[d, part, :] = decay
            direct_ref[d, part, :] = root * inward
            inward_ref[d, part, :] = root * gated * (1.0 - inward)
            slope = decay * (state - gated * decay / root)
            recur_ref[d, part, :] = -(slope * speed) * (recur * (1.0 - recur))
        x = branch_ref[part, :].astype(f32)
        c = 0.7978845608028654
        t = jnp.tanh(c * (x + 0.044715 * (x * x * x)))
        gelu = 0.5 * x * (1.0 + t)
        slope = 0.5 * (1.0 + t) + 0.5 * x * (1.0 - t * t) * (c * (1.0 + 0.134145 * (x * x)))
        mix_ref[part, :] = (lru * gelu).astype(bf16)
        gelu_ref[part, :] = gelu
        back_ref[part, :] = lru * slope


def project_kernel(ranks, experts, tp_ref, sp_ref, mix_ref, *refs):
    parts, outs, buf = refs[:ranks], refs[ranks : ranks + experts], refs[-1]
    width = parts[0].shape[1]
    across = buf.shape[2]
    mix = mix_ref[...]
    for r in range(ranks):
        value = dot(mix, parts[r][...], nn).astype(bf16)
        for j in range(width // across):
            buf[(tp_ref[0] ^ r) * (width // across) + j] = value[:, j * across : (j + 1) * across]
    for s in range(experts):
        outs[s][...] = buf[sp_ref[0] ^ s]


def scan_kernel(ranks, place_ref, proj_ref, gelu_ref, back_ref, decay_ref, *refs):
    parts = refs[:ranks]
    branch_ref, local_ref, reach_ref, ends_ref, grad_ref = refs[ranks:]
    width = parts[0].shape[1]
    place = place_ref[0]
    total = None
    for r in range(ranks):
        where = pl.ds(pl.multiple_of((place ^ r) * width, width), width)
        one = dot(proj_ref[:, where], parts[r][...], nt)
        total = one if r == 0 else total + one
    grad_ref[...] = total
    channels, length = gelu_ref.shape
    size = min(64, channels)
    for b in range(channels // size):
        part = slice(b * size, (b + 1) * size)
        mix_grad = grad_ref[part, :]
        lru_grad = mix_grad * gelu_ref[part, :]
        branch_ref[part, :] = mix_grad * back_ref[part, :]
        lane = lax.broadcasted_iota(jnp.int32, (size, 128), 1)
        ends = jnp.zeros((size, 128), f32)
        for d in range(2):
            reverse = d == 0
            prod = decay_ref[d, part, :]
            local = prod * lru_grad
            step = 1
            while step < length:
                local = local + prod * shifted(local, step, reverse, 0.0)
                prod = prod * shifted(prod, step, reverse, 1.0)
                step *= 2
            last = slice(0, 1) if reverse else slice(length - 1, length)
            ends = jnp.where(lane == 2 * d, prod[:, last], ends)
            ends = jnp.where(lane == 2 * d + 1, local[:, last], ends)
            local_ref[d, part, :] = lru_grad + shifted(local, 1, reverse, 0.0)
            reach_ref[d, part, :] = shifted(prod, 1, reverse, 1.0)
        ends_ref[:, part] = ends.T[:8]


def finish_kernel(
    place_ref, ends_ref, local_ref, reach_ref, direct_ref, recur_ref, inward_ref,
    recur_maps, input_maps, out_ref,
):
    count, _, channels = ends_ref.shape
    place = place_ref[0]
    ahead = jnp.zeros((1, channels), f32)
    behind = jnp.zeros((1, channels), f32)
    for e in range(count):
        back = ends_ref[e, 2:3] * behind + ends_ref[e, 3:4]
        behind = jnp.where(e < place, back, behind)
        e = count - 1 - e
        fore = ends_ref[e, 0:1] * ahead + ends_ref[e, 1:2]
        ahead = jnp.where(e > place, fore, ahead)
    row = lax.broadcasted_iota(jnp.int32, (128, channels), 0)
    both = jnp.where(row == 0, ahead, jnp.where(row == 1, behind, 0.0)).T
    blocks, size = recur_maps.shape[1], recur_maps.shape[2]
    for b in range(blocks):
        part = slice(b * size, (b + 1) * size)
        total = None
        for d in range(2):
            delta = local_ref[d, part, :] + reach_ref[d, part, :] * both[part, d : d + 1]
            direct = delta * direct_ref[d, part, :]
            total = direct if d == 0 else total + direct
            for maps, slopes in ((recur_maps, recur_ref), (input_maps, inward_ref)):
                wide = delta * slopes[d, part, :]
                high = wide.astype(bf16)
                low = (wide - high.astype(f32)).astype(bf16)
                total = total + (dot(maps[d, b], high, nn) + dot(maps[d, b], low, nn))
        out_ref[part, :] = total


def swap(value, axis, bit):
    count = lax.axis_size(axis)
    return lax.ppermute(value, axis, [(i, i ^ bit) for i in range(count)])


def rank_bits(ranks):
    bits = [1 << b for b in range(1, ranks.bit_length() - 1)]
    return bits + [1] if ranks > 1 else []


def gather_parts(own):
    ranks = lax.axis_size("tp")
    parts = {0: own}
    for bit in rank_bits(ranks):
        for r in list(parts):
            parts[r | bit] = swap(parts[r], "tp", bit)
    return [parts[r] for r in range(ranks)]


def sum_parts(keep, send):
    got = swap(send, "tp", 1)
    ranks = lax.axis_size("tp")
    value = keep.astype(f32) + got.astype(f32)
    bit = 2
    while bit < ranks:
        half = value.shape[0] // 2
        got = swap(value[half:].astype(bf16), "tp", bit)
        value = value[:half] + got.astype(f32)
        if 2 * bit == ranks:
            return value[0].astype(bf16)
        bit *= 2
    return value[0].astype(bf16)


def chunk_plan(experts):
    unit = max(1, experts // 8)
    return [list(range(a, a + unit)) for a in range(0, experts, unit)], [[0, 1], [2, 3], [4, 5], [6, 7]]


def scheduled(
    cotangent, moe_input, routes, gates, w_gate, w_up, w_down, out_proj,
    conv_in, branch, state_before, state_after, jump, recur_weight, input_weight, lam,
):
    tokens, width = cotangent.shape
    top = routes.shape[1]
    experts = lax.axis_size("sp")
    ranks = lax.axis_size("tp")
    capacity = 3 * tokens // experts
    features = width * ranks
    hidden = w_gate.shape[2]
    channels, length = conv_in.shape
    sp = lax.axis_index("sp").astype(jnp.int32).reshape(1)
    tp = lax.axis_index("tp").astype(jnp.int32).reshape(1)

    inputs = (routes.T, gates.T, moe_input, cotangent)
    packed = call(
        functools.partial(pack_kernel, experts, capacity),
        (sp, *inputs),
        [shape((tokens, 2 * top), jnp.int32)]
        + [shape((capacity, 2 * width), bf16) for _ in range(experts)],
        scratch=[pltpu.VMEM(a.shape, a.dtype) for a in inputs]
        + [pltpu.SemaphoreType.DMA((len(inputs),))],
        flops=6 * tokens * experts * capacity * width,
        free=4,
        grant=60,
    )
    table, blocks = packed[0], packed[1:]

    plane = shape((channels, length), f32)
    pair = shape((2, channels, length), f32)
    gate_inputs = (
        recur_weight, input_weight, lam, conv_in, state_before, state_after, jump, branch,
    )
    gate_outs = (shape((channels, length), bf16), plane, plane, pair, pair, pair, pair)
    mix, gelu_val, gelu_back, decay, direct, recur, inward = call(
        gates_kernel, gate_inputs, gate_outs, flops=400 * channels * length, scalars=0, grant=12
    )

    turn = ticket(tp, 40 * tokens * features * hidden)
    weights = (w_gate[0], w_up[0], w_down[0])
    chunks, groups = chunk_plan(experts)
    arrived = [blocks[0]]
    arrived += [swap(blocks[s], "sp", s) for s in range(1, experts)]
    parts = []
    for sources in chunks:
        own = [arrived[s] for s in sources]
        own = own[0] if len(own) == 1 else jnp.concatenate(own, axis=0)
        parts.append(gather_parts(own))
    hiddens, returned = [], [None] * experts
    for members in groups:
        sources = [s for c in members for s in chunks[c]]
        group_rows = len(sources) * capacity
        part_kind = shape((ranks // 2, group_rows, width), bf16)
        hid_kind = shape((group_rows, hidden), bf16)
        keep, send, *hids = call(
            functools.partial(expert_kernel, ranks, len(members)),
            (turn, *[part for c in members for part in parts[c]], *weights),
            [part_kind, part_kind, hid_kind, hid_kind, hid_kind],
            flops=10 * group_rows * features * hidden,
        )
        hiddens.append(hids)
        row_grad = sum_parts(keep, send)
        for i, s in enumerate(sources):
            block = row_grad[i * capacity : (i + 1) * capacity]
            returned[s] = swap(block, "sp", s) if s else block

    every = (tp, *[p for part in parts for p in part])
    sizes = (ranks, len(chunks), len(groups))

    def weight_call(kernel, hids, outs, scratch):
        return pl.pallas_call(
            functools.partial(kernel, *sizes),
            out_shape=tuple(outs),
            in_specs=[pl.BlockSpec(memory_space=pltpu.SMEM)]
            + [pl.BlockSpec(memory_space=pltpu.VMEM)] * (len(every) - 1 + len(hids)),
            out_specs=tuple(pl.BlockSpec(memory_space=pl.ANY) for _ in outs),
            scratch_shapes=[pltpu.VMEM(dims, bf16) for dims in scratch]
            + [pltpu.SemaphoreType.DMA((2, ranks) if len(outs) > 1 else (ranks,))],
            cost_estimate=pl.CostEstimate(
                flops=2 * len(outs) * experts * capacity * features * hidden,
                bytes_accessed=2 * features * (hidden + experts * capacity),
                transcendentals=0,
            ),
            compiler_params=pltpu.CompilerParams(vmem_limit_bytes=16 * 1024 * 1024),
        )(*every, *hids)

    row_dims, col_dims = (features, hidden), (hidden, features)
    gate_grad, up_grad = weight_call(
        weight_kernel,
        [hids[j] for j in (1, 2) for hids in hiddens],
        [shape(row_dims, bf16)] * 2,
        [(ranks, width, hidden)] * 2,
    )
    (down_grad,) = weight_call(
        down_kernel,
        [hids[0] for hids in hiddens],
        [shape(col_dims, bf16)],
        [(ranks, hidden, width)],
    )

    (residual_grad,) = call(
        functools.partial(combine_kernel, experts),
        (sp, table, cotangent, *returned),
        [shape((tokens, width), bf16)],
        flops=2 * tokens * experts * capacity * width,
        grant=12,
    )
    full = gather_parts(residual_grad)
    across = features // experts
    block = shape((channels, across), bf16)
    projected = call(
        functools.partial(project_kernel, ranks, experts),
        (tp, sp, mix, *full),
        [block] * experts,
        scratch=[pltpu.VMEM((experts, channels, across), bf16)],
        flops=2 * channels * tokens * features,
        scalars=2,
        grant=12,
    )
    exchanged = [projected[0]]
    exchanged += [swap(projected[s], "sp", s) for s in range(1, experts)]
    branch_grad, local, reach, ends = call(
        functools.partial(scan_kernel, ranks),
        (tp, out_proj, gelu_val, gelu_back, decay, *full),
        [plane, pair, pair, shape((8, channels), f32)],
        scratch=[pltpu.VMEM((channels, length), f32)],
        flops=2 * channels * tokens * features,
        grant=12,
    )
    all_ends = lax.all_to_all(
        jnp.broadcast_to(ends[None], (experts, *ends.shape)), "sp", 0, 0, tiled=True
    )
    (conv_grad,) = call(
        finish_kernel,
        (sp, all_ends, local, reach, direct, recur, inward, recur_weight, input_weight),
        [plane],
        flops=400 * channels * length,
        grant=12,
    )
    out_proj_grad = functools.reduce(jnp.add, [part.astype(f32) for part in exchanged])
    return (
        gate_grad[None], up_grad[None], down_grad[None], residual_grad,
        out_proj_grad, conv_grad, branch_grad,
    )


def solution(mesh):
    placed = (
        P("sp", "tp"), P("sp", "tp"), P("sp", None), P("sp", None),
        P("sp", None, "tp"), P("sp", None, "tp"), P("sp", "tp", None), P("tp", None),
        P("tp", "sp"), P("tp", "sp"), P("tp", "sp"), P("tp", "sp"), P("tp", "sp"),
        P(None, "tp", None, None), P(None, "tp", None, None), P(None, "tp"),
    )
    return jax.shard_map(
        scheduled,
        mesh=mesh,
        in_specs=placed,
        out_specs=(
            P("sp", None, "tp"), P("sp", None, "tp"), P("sp", "tp", None), P("sp", "tp"),
            P("tp", "sp"), P("tp", "sp"), P("tp", "sp"),
        ),
        check_vma=False,
    )
```

profile of v0, /device:TPU:0, one launch (start us, length us, event | category | flops | bytes accessed | tf_op | source)
XLA Modules:
  0.0 204.5 jit_solution(4479387058130932749)
XLA Ops:
  0.6 4.0 %shard_map.207 = (s32[256,4]{1,0:T(8,128)}, bf16[96,1024]{1,0:T(8,128)(2,1)}, bf16[96,1024]{1,0:T(8,128)(2,1)}, bf16[96,1024]{1,0:T(8,128)(2,1)}, bf16[96,1024]{...) custom-call(s32[1]{0:T(128)} %bitcast.1.place_ref.sp_ref, ...), custom_call_target="tpu_custom_call" | custom-call | flops 603979776 | bytes 2105348 | tf_op jit(solution)/shard_map/pallas_call | solution.py:31
  4.7 5.1 %collective-permute-start.23 = (bf16[96,1024]{1,0:T(8,128)(2,1)}, bf16[96,1024]{1,0:T(8,128)(2,1)S(1)}, u32[]{:S(2)}, u32[]{:S(2)}) collective-permute-start(bf16[96,1024]{1,0:T(8,128)(2,1)} %get-tuple-element.63), channel_id=1, source_target_pairs={{0,24},{4,28},{8,16},{12,20},{16,8},{20,12},{24,0},{28,4},{1,25},{... | collective-permute-start | bytes 589832 | tf_op jit(solution)/shard_map/ppermute | solution.py:373
  15.4 17.9 %collective-permute-start.11 = (bf16[96,1024]{1,0:T(8,128)(2,1)}, bf16[96,1024]{1,0:T(8,128)(2,1)S(1)}, u32[]{:S(2)}, u32[]{:S(2)}) collective-permute-start(bf16[96,1024]{1,0:T(8,128)(2,1)} %get-tuple-element.60), channel_id=1, source_target_pairs={{0,12},{4,8},{8,4},{12,0},{16,28},{20,24},{24,20},{28,16},{1,13},{... | collective-permute-start | bytes 589832 | tf_op jit(solution)/shard_map/ppermute | solution.py:373
  33.9 6.5 %collective-permute-done.15.refs_0_.refs_16_ = bf16[96,1024]{1,0:T(8,128)(2,1)S(1)} collective-permute-done((bf16[96,1024]{1,0:T(8,128)(2,1)}, bf16[96,1024]{1,0:T(8,128)(2,1)S(1)}, u32[]{:S(2)}, u32[]{:S(2)}) %collective-permute-start.15) | collective-permute-done | bytes 196640 | tf_op jit(solution)/shard_map/ppermute | solution.py:373
  41.9 2.9 %collective-permute-done.19.refs_4_.refs_20_ = bf16[96,1024]{1,0:T(8,128)(2,1)S(1)} collective-permute-done((bf16[96,1024]{1,0:T(8,128)(2,1)}, bf16[96,1024]{1,0:T(8,128)(2,1)S(1)}, u32[]{:S(2)}, u32[]{:S(2)}) %collective-permute-start.19) | collective-permute-done | bytes 196640 | tf_op jit(solution)/shard_map/ppermute | solution.py:373
  48.8 3.7 %collective-permute-done.25.refs_2_.refs_26_ = bf16[96,1024]{1,0:T(8,128)(2,1)S(1)} collective-permute-done((bf16[96,1024]{1,0:T(8,128)(2,1)S(1)}, bf16[96,1024]{1,0:T(8,128)(2,1)S(1)}, u32[]{:S(2)}, u32[]{:S(2)}) %collective-permute-start.25) | collective-permute-done | bytes 196640 | tf_op jit(solution)/shard_map/ppermute | solution.py:373
  54.1 2.7 %collective-permute-done.29.refs_6_.refs_30_ = bf16[96,1024]{1,0:T(8,128)(2,1)S(1)} collective-permute-done((bf16[96,1024]{1,0:T(8,128)(2,1)S(1)}, bf16[96,1024]{1,0:T(8,128)(2,1)S(1)}, u32[]{:S(2)}, u32[]{:S(2)}) %collective-permute-start.29) | collective-permute-done | bytes 196640 | tf_op jit(solution)/shard_map/ppermute | solution.py:373
  58.8 2.2 %collective-permute-done.17.refs_2_.refs_18_ = bf16[96,1024]{1,0:T(8,128)(2,1)S(1)} collective-permute-done((bf16[96,1024]{1,0:T(8,128)(2,1)S(1)}, bf16[96,1024]{1,0:T(8,128)(2,1)S(1)}, u32[]{:S(2)}, u32[]{:S(2)}) %collective-permute-start.17) | collective-permute-done | bytes 196640 | tf_op jit(solution)/shard_map/ppermute | solution.py:373
  62.5 2.7 %collective-permute-done.21.refs_6_.refs_22_ = bf16[96,1024]{1,0:T(8,128)(2,1)S(1)} collective-permute-done((bf16[96,1024]{1,0:T(8,128)(2,1)S(1)}, bf16[96,1024]{1,0:T(8,128)(2,1)S(1)}, u32[]{:S(2)}, u32[]{:S(2)}) %collective-permute-start.21) | collective-permute-done | bytes 196640 | tf_op jit(solution)/shard_map/ppermute | solution.py:373
  65.8 3.7 %collective-permute-done.9.refs_2_.refs_10_ = bf16[96,1024]{1,0:T(8,128)(2,1)} collective-permute-done((bf16[96,1024]{1,0:T(8,128)(2,1)S(1)}, bf16[96,1024]{1,0:T(8,128)(2,1)}, u32[]{:S(2)}, u32[]{:S(2)}) %collective-permute-start.9) | collective-permute-done | bytes 196640 | tf_op jit(solution)/shard_map/ppermute | solution.py:373
  69.5 2.4 %collective-permute-done.13.refs_6_.refs_14_ = bf16[96,1024]{1,0:T(8,128)(2,1)} collective-permute-done((bf16[96,1024]{1,0:T(8,128)(2,1)S(1)}, bf16[96,1024]{1,0:T(8,128)(2,1)}, u32[]{:S(2)}, u32[]{:S(2)}) %collective-permute-start.13) | collective-permute-done | bytes 196640 | tf_op jit(solution)/shard_map/ppermute | solution.py:373
  77.3 5.5 %shard_map.211 = (bf16[2,192,512]{2,1,0:T(8,128)(2,1)S(1)}, bf16[2,192,512]{2,1,0:T(8,128)(2,1)S(1)}, bf16[192,512]{1,0:T(8,128)(2,1)S(1)}, bf16[192,512]{1,0:T(8,128)(2,1)S(1)}, bf16[192,512]{1,0:T(8,128)(2,1)S(1)}) custom-call(s32[1]{0:T(128)} %ticket.1.place_ref, bf16[96,1024]{1,0:T(8,128)(2,1)S(1)} %collective-permute-done.23.refs_0_.refs_24_, ...), custom_call_target="tpu_custom_call" | custom-call | flops 2013265920 | bytes 9240580 | tf_op jit(solution)/shard_map/pallas_call | solution.py:31
  84.8 4.5 %shard_map.210 = (bf16[2,192,512]{2,1,0:T(8,128)(2,1)S(1)}, bf16[2,192,512]{2,1,0:T(8,128)(2,1)S(1)}, bf16[192,512]{1,0:T(8,128)(2,1)S(1)}, bf16[192,512]{1,0:T(8,128)(2,1)S(1)}, bf16[192,512]{1,0:T(8,128)(2,1)S(1)}) custom-call(s32[1]{0:T(128)} %ticket.1.place_ref, bf16[96,1024]{1,0:T(8,128)(2,1)S(1)} %collective-permute-done.15.refs_0_.refs_16_, ...), custom_call_target="tpu_custom_call" | custom-call | flops 2013265920 | bytes 9240580 | tf_op jit(solution)/shard_map/pallas_call | solution.py:31
  89.3 5.6 %shard_map.209 = (bf16[2,192,512]{2,1,0:T(8,128)(2,1)S(1)}, bf16[2,192,512]{2,1,0:T(8,128)(2,1)S(1)}, bf16[192,512]{1,0:T(8,128)(2,1)S(1)}, bf16[192,512]{1,0:T(8,128)(2,1)S(1)}, bf16[192,512]{1,0:T(8,128)(2,1)S(1)}) custom-call(s32[1]{0:T(128)} %ticket.1.place_ref, bf16[96,1024]{1,0:T(8,128)(2,1)S(1)} %collective-permute-done.7.refs_0_.refs_8_, ...), custom_call_target="tpu_custom_call" | custom-call | flops 2013265920 | bytes 9240580 | tf_op jit(solution)/shard_map/pallas_call | solution.py:31
  95.7 4.5 %shard_map.208 = (bf16[2,192,512]{2,1,0:T(8,128)(2,1)S(1)}, bf16[2,192,512]{2,1,0:T(8,128)(2,1)S(1)}, bf16[192,512]{1,0:T(8,128)(2,1)S(1)}, bf16[192,512]{1,0:T(8,128)(2,1)S(1)}, bf16[192,512]{1,0:T(8,128)(2,1)S(1)}) custom-call(s32[1]{0:T(128)} %ticket.1.place_ref, bf16[96,1024]{1,0:T(8,128)(2,1)S(1)} %copy-done.6, ...), custom_call_target="tpu_custom_call" | custom-call | flops 2013265920 | bytes 9240580 | tf_op jit(solution)/shard_map/pallas_call | solution.py:31
  105.6 3.1 %collective-permute-done.43 = bf16[1,192,512]{2,1,0:T(8,128)(2,1)S(1)} collective-permute-done((bf16[1,192,512]{2,1,0:T(8,128)(2,1)S(1)}, bf16[1,192,512]{2,1,0:T(8,128)(2,1)S(1)}, u32[]{:S(2)}, u32[]{:S(2)}) %collective-permute-start.43) | collective-permute-done | bytes 196640 | tf_op jit(solution)/shard_map/ppermute | solution.py:373
  108.7 2.5 %collective-permute-start.44 = (bf16[96,512]{1,0:T(8,128)(2,1)S(1)}, bf16[96,512]{1,0:T(8,128)(2,1)S(1)}, u32[]{:S(2)}, u32[]{:S(2)}) collective-permute-start(bf16[96,512]{1,0:T(8,128)(2,1)S(1)} %get-tuple-element.108), channel_id=1, source_target_pairs={{0,24},{4,28},{8,16},{12,20},{16,8},{20,12},{24,0},{28,4},{1,25},{... | collective-permute-start | bytes 294920 | tf_op jit(solution)/shard_map/ppermute | solution.py:373
  111.3 2.3 %collective-permute-start.45 = (bf16[96,512]{1,0:T(8,128)(2,1)S(1)}, bf16[96,512]{1,0:T(8,128)(2,1)S(1)}, u32[]{:S(2)}, u32[]{:S(2)}) collective-permute-start(bf16[96,512]{1,0:T(8,128)(2,1)S(1)} %get-tuple-element.107), channel_id=1, source_target_pairs={{0,28},{4,24},{8,20},{12,16},{16,12},{20,8},{24,4},{28,0},{1,29},{... | collective-permute-start | bytes 294920 | tf_op jit(solution)/shard_map/ppermute | solution.py:373
  113.8 3.3 %collective-permute-done.35 = bf16[1,192,512]{2,1,0:T(8,128)(2,1)S(1)} collective-permute-done((bf16[1,192,512]{2,1,0:T(8,128)(2,1)S(1)}, bf16[1,192,512]{2,1,0:T(8,128)(2,1)S(1)}, u32[]{:S(2)}, u32[]{:S(2)}) %collective-permute-start.35) | collective-permute-done | bytes 196640 | tf_op jit(solution)/shard_map/ppermute | solution.py:373
  118.2 2.4 %collective-permute-done.32 = bf16[1,192,512]{2,1,0:T(8,128)(2,1)S(1)} collective-permute-done((bf16[1,192,512]{2,1,0:T(8,128)(2,1)S(1)}, bf16[1,192,512]{2,1,0:T(8,128)(2,1)S(1)}, u32[]{:S(2)}, u32[]{:S(2)}) %collective-permute-start.32) | collective-permute-done | bytes 196640 | tf_op jit(solution)/shard_map/ppermute | solution.py:373
  125.2 2.5 %collective-permute-done.41.refs_5_ = bf16[96,512]{1,0:T(8,128)(2,1)S(1)} collective-permute-done((bf16[96,512]{1,0:T(8,128)(2,1)S(1)}, bf16[96,512]{1,0:T(8,128)(2,1)S(1)}, u32[]{:S(2)}, u32[]{:S(2)}) %collective-permute-start.41) | collective-permute-done | bytes 98336 | tf_op jit(solution)/shard_map/ppermute | solution.py:373
  128.7 2.5 %collective-permute-done.37.refs_3_ = bf16[96,512]{1,0:T(8,128)(2,1)S(1)} collective-permute-done((bf16[96,512]{1,0:T(8,128)(2,1)S(1)}, bf16[96,512]{1,0:T(8,128)(2,1)S(1)}, u32[]{:S(2)}, u32[]{:S(2)}) %collective-permute-start.37) | collective-permute-done | bytes 98336 | tf_op jit(solution)/shard_map/ppermute | solution.py:373
  133.4 7.5 %collective-permute-done.47.refs_2_ = bf16[256,512]{1,0:T(8,128)(2,1)S(1)} collective-permute-done((bf16[256,512]{1,0:T(8,128)(2,1)}, bf16[256,512]{1,0:T(8,128)(2,1)S(1)}, u32[]{:S(2)}, u32[]{:S(2)}) %collective-permute-start.47) | collective-permute-done | bytes 262176 | tf_op jit(solution)/shard_map/ppermute | solution.py:373
  148.6 5.8 %shard_map.212 = (bf16[2048,512]{1,0:T(8,128)(2,1)}, bf16[2048,512]{1,0:T(8,128)(2,1)}) custom-call(s32[1]{0:T(128)} %bitcast.place_ref.tp_ref, bf16[96,1024]{1,0:T(8,128)(2,1)S(1)} %copy-done.6, bf16[96,1024]{1,0:T(8,128)(2,1)S(1)} %collective-permute-done.refs_1_, bf16[96,1024]{1,0:T(8,128)(2,1)S(1)} %collective-permute-done.1.refs_2_, ...), custom_call_target="tpu_custom_call" | custom-call | flops 3221225472 | bytes 5242880 | tf_op jit(solution)/shard_map/pallas_call | solution.py:481
  154.4 5.5 %shard_map.217 = (f32[256,256]{1,0:T(8,128)}, f32[2,256,256]{2,1,0:T(8,128)S(1)}, f32[2,256,256]{2,1,0:T(8,128)S(1)}, f32[8,256]{1,0:T(8,128)S(1)}) custom-call(s32[1]{0:T(128)} %bitcast.place_ref.tp_ref, bf16[256,2048]{1,0:T(8,128)(2,1)S(1)} %copy-done.5, f32[256,256]{1,0:T(8,128)S(1)} %get-tuple-element.97.gelu_ref, ...), custom_call_target="tpu_custom_call" | custom-call | flops 268435456 | bytes 4464644 | tf_op jit(solution)/shard_map/pallas_call | solution.py:31
  162.1 5.1 %all-to-all-start = ((f32[8,8,256]{2,1,0:T(8,128)}), f32[8,8,256]{2,1,0:T(8,128)S(1)}, u32[]{:S(2)}, u32[]{:S(2)}) async-start(f32[8,8,256]{2,1,0:T(8,128)} %broadcast_in_dim.18), calls=%async_computation | async-start | bytes 131072 | tf_op jit(solution)/shard_map/all_to_all | solution.py:540
  167.3 2.9 %collective-permute-start.51 = (bf16[256,256]{1,0:T(8,128)(2,1)}, bf16[256,256]{1,0:T(8,128)(2,1)}, u32[]{:S(2)}, u32[]{:S(2)}) collective-permute-start(bf16[256,256]{1,0:T(8,128)(2,1)} %copy-done.65), channel_id=1, source_target_pairs={{0,12},{4,8},{8,4},{12,0},{16,28},{20,24},{24,20},{28,16},{1,13},{... | collective-permute-start | bytes 393224 | tf_op jit(solution)/shard_map/ppermute | solution.py:373
  170.2 2.4 %collective-permute-start.52 = (bf16[256,256]{1,0:T(8,128)(2,1)}, bf16[256,256]{1,0:T(8,128)(2,1)}, u32[]{:S(2)}, u32[]{:S(2)}) collective-permute-start(bf16[256,256]{1,0:T(8,128)(2,1)} %copy-done.64), channel_id=1, source_target_pairs={{0,16},{4,20},{8,24},{12,28},{16,0},{20,4},{24,8},{28,12},{1,17},{... | collective-permute-start | bytes 393224 | tf_op jit(solution)/shard_map/ppermute | solution.py:373
  173.1 2.4 %collective-permute-start.54 = (bf16[256,256]{1,0:T(8,128)(2,1)}, bf16[256,256]{1,0:T(8,128)(2,1)}, u32[]{:S(2)}, u32[]{:S(2)}) collective-permute-start(bf16[256,256]{1,0:T(8,128)(2,1)} %copy-done.62), channel_id=1, source_target_pairs={{0,24},{4,28},{8,16},{12,20},{16,8},{20,12},{24,0},{28,4},{1,25},{... | collective-permute-start | bytes 393224 | tf_op jit(solution)/shard_map/ppermute | solution.py:373
  175.5 2.4 %collective-permute-start.55 = (bf16[256,256]{1,0:T(8,128)(2,1)}, bf16[256,256]{1,0:T(8,128)(2,1)}, u32[]{:S(2)}, u32[]{:S(2)}) collective-permute-start(bf16[256,256]{1,0:T(8,128)(2,1)} %copy-done.61), channel_id=1, source_target_pairs={{0,28},{4,24},{8,20},{12,16},{16,12},{20,8},{24,4},{28,0},{1,29},{... | collective-permute-start | bytes 393224 | tf_op jit(solution)/shard_map/ppermute | solution.py:373
  191.8 4.0 %shard_map.213 = bf16[512,2048]{1,0:T(8,128)(2,1)} custom-call(s32[1]{0:T(128)} %bitcast.place_ref.tp_ref, bf16[96,1024]{1,0:T(8,128)(2,1)S(1)} %copy-done.6, bf16[96,1024]{1,0:T(8,128)(2,1)S(1)} %copy-done.24, bf16[96,1024]{1,0:T(8,128)(2,1)S(1)} %collective-permute-done.1.refs_2_, bf16[96,1024]{1,0:T(8,128)(2,1)S(1)} %copy-done.28, ...), custom_call_target="tpu_custom_call" | custom-call | flops 1610612736 | bytes 5242880 | tf_op jit(solution)/shard_map/pallas_call | solution.py:481
  202.4 2.1 %convert_add_fusion.4 = f32[256,256]{1,0:T(8,128)} fusion(bf16[256,256]{1,0:T(8,128)(2,1)} %collective-permute-done.55, bf16[256,256]{1,0:T(8,128)(2,1)} %collective-permute-done.54, bf16[256,256]{1,0:T(8,128)(2,1)} %collective-permute-done.53, bf16[256,256]{1,0:T(8,128)(2,1)} %collective-permute-done.52, bf16[256,256]{1,0:T(8,128)(2,1)} %collective-permute-done.51, ...), kind=kLoop, calls=%fused_computation.16 | loop fusion | flops 983040 | bytes 1310720 | tf_op jit(solution)/shard_map/add | solution.py:550
  (245 shorter events, 70.6 us)
Async XLA Ops:
  4.7 10.8 %collective-permute-start.23 = (bf16[96,1024]{1,0:T(8,128)(2,1)}, bf16[96,1024]{1,0:T(8,128)(2,1)S(1)}, u32[]{:S(2)}, u32[]{:S(2)}) collective-permute-start(bf16[96,1024]{1,0:T(8,128)(2,1)} %get-tuple-element.63), channel_id=1, source_target_pairs={{0,24},{4,28},{8,16},{12,20},{16,8},{20,12},{24,0},{28,4},{1,25},{... | collective-permute-start | bytes 589832 | tf_op jit(solution)/shard_map/ppermute | solution.py:373
  9.8 23.6 %collective-permute-start.27 = (bf16[96,1024]{1,0:T(8,128)(2,1)}, bf16[96,1024]{1,0:T(8,128)(2,1)S(1)}, u32[]{:S(2)}, u32[]{:S(2)}) collective-permute-start(bf16[96,1024]{1,0:T(8,128)(2,1)} %get-tuple-element.64), channel_id=1, source_target_pairs={{0,28},{4,24},{8,20},{12,16},{16,12},{20,8},{24,4},{28,0},{1,29},{... | collective-permute-start | bytes 589832 | tf_op jit(solution)/shard_map/ppermute | solution.py:373
  10.9 29.4 %collective-permute-start.15 = (bf16[96,1024]{1,0:T(8,128)(2,1)}, bf16[96,1024]{1,0:T(8,128)(2,1)S(1)}, u32[]{:S(2)}, u32[]{:S(2)}) collective-permute-start(bf16[96,1024]{1,0:T(8,128)(2,1)} %get-tuple-element.61), channel_id=1, source_target_pairs={{0,16},{4,20},{8,24},{12,28},{16,0},{20,4},{24,8},{28,12},{1,17},{... | collective-permute-start | bytes 589832 | tf_op jit(solution)/shard_map/ppermute | solution.py:373
  11.7 33.1 %collective-permute-start.19 = (bf16[96,1024]{1,0:T(8,128)(2,1)}, bf16[96,1024]{1,0:T(8,128)(2,1)S(1)}, u32[]{:S(2)}, u32[]{:S(2)}) collective-permute-start(bf16[96,1024]{1,0:T(8,128)(2,1)} %get-tuple-element.62), channel_id=1, source_target_pairs={{0,20},{4,16},{8,28},{12,24},{16,4},{20,0},{24,12},{28,8},{1,21},{... | collective-permute-start | bytes 589832 | tf_op jit(solution)/shard_map/ppermute | solution.py:373
  13.7 32.6 %collective-permute-start.7 = (bf16[96,1024]{1,0:T(8,128)(2,1)}, bf16[96,1024]{1,0:T(8,128)(2,1)S(1)}, u32[]{:S(2)}, u32[]{:S(2)}) collective-permute-start(bf16[96,1024]{1,0:T(8,128)(2,1)} %get-tuple-element.59), channel_id=1, source_target_pairs={{0,8},{4,12},{8,0},{12,4},{16,24},{20,28},{24,16},{28,20},{1,9},{5... | collective-permute-start | bytes 589832 | tf_op jit(solution)/shard_map/ppermute | solution.py:373
  15.4 31.4 %collective-permute-start.11 = (bf16[96,1024]{1,0:T(8,128)(2,1)}, bf16[96,1024]{1,0:T(8,128)(2,1)S(1)}, u32[]{:S(2)}, u32[]{:S(2)}) collective-permute-start(bf16[96,1024]{1,0:T(8,128)(2,1)} %get-tuple-element.60), channel_id=1, source_target_pairs={{0,12},{4,8},{8,4},{12,0},{16,28},{20,24},{24,20},{28,16},{1,13},{... | collective-permute-start | bytes 589832 | tf_op jit(solution)/shard_map/ppermute | solution.py:373
  33.4 13.5 %collective-permute-start.3 = (bf16[96,1024]{1,0:T(8,128)(2,1)}, bf16[96,1024]{1,0:T(8,128)(2,1)S(1)}, u32[]{:S(2)}, u32[]{:S(2)}) collective-permute-start(bf16[96,1024]{1,0:T(8,128)(2,1)} %get-tuple-element.58), channel_id=1, source_target_pairs={{0,4},{4,0},{8,12},{12,8},{16,20},{20,16},{24,28},{28,24},{1,5},{5... | collective-permute-start | bytes 589832 | tf_op jit(solution)/shard_map/ppermute | solution.py:373
  47.4 13.6 %collective-permute-start.17 = (bf16[96,1024]{1,0:T(8,128)(2,1)S(1)}, bf16[96,1024]{1,0:T(8,128)(2,1)S(1)}, u32[]{:S(2)}, u32[]{:S(2)}) collective-permute-start(bf16[96,1024]{1,0:T(8,128)(2,1)S(1)} %collective-permute-done.15.refs_0_.refs_16_), channel_id=1, source_target_pairs={{0,2},{1,3},{2,0},{3,1},{4,6},{5,7},{6,4},{7,5},{8,10},{9,11},{10,... | collective-permute-start | bytes 589832 | tf_op jit(solution)/shard_map/ppermute | solution.py:373
  52.6 12.6 %collective-permute-start.21 = (bf16[96,1024]{1,0:T(8,128)(2,1)S(1)}, bf16[96,1024]{1,0:T(8,128)(2,1)S(1)}, u32[]{:S(2)}, u32[]{:S(2)}) collective-permute-start(bf16[96,1024]{1,0:T(8,128)(2,1)S(1)} %collective-permute-done.19.refs_4_.refs_20_), channel_id=1, source_target_pairs={{0,2},{1,3},{2,0},{3,1},{4,6},{5,7},{6,4},{7,5},{8,10},{9,11},{10,... | collective-permute-start | bytes 589832 | tf_op jit(solution)/shard_map/ppermute | solution.py:373
  57.3 12.2 %collective-permute-start.9 = (bf16[96,1024]{1,0:T(8,128)(2,1)S(1)}, bf16[96,1024]{1,0:T(8,128)(2,1)}, u32[]{:S(2)}, u32[]{:S(2)}) collective-permute-start(bf16[96,1024]{1,0:T(8,128)(2,1)S(1)} %collective-permute-done.7.refs_0_.refs_8_), channel_id=1, source_target_pairs={{0,2},{1,3},{2,0},{3,1},{4,6},{5,7},{6,4},{7,5},{8,10},{9,11},{10,... | collective-permute-start | bytes 589832 | tf_op jit(solution)/shard_map/ppermute | solution.py:373
  61.0 10.9 %collective-permute-start.13 = (bf16[96,1024]{1,0:T(8,128)(2,1)S(1)}, bf16[96,1024]{1,0:T(8,128)(2,1)}, u32[]{:S(2)}, u32[]{:S(2)}) collective-permute-start(bf16[96,1024]{1,0:T(8,128)(2,1)S(1)} %collective-permute-done.11.refs_4_.refs_12_), channel_id=1, source_target_pairs={{0,2},{1,3},{2,0},{3,1},{4,6},{5,7},{6,4},{7,5},{8,10},{9,11},{10,... | collective-permute-start | bytes 589832 | tf_op jit(solution)/shard_map/ppermute | solution.py:373
  71.9 11.6 %collective-permute-start.5 = (bf16[96,1024]{1,0:T(8,128)(2,1)S(1)}, bf16[96,1024]{1,0:T(8,128)(2,1)S(1)}, u32[]{:S(2)}, u32[]{:S(2)}) collective-permute-start(bf16[96,1024]{1,0:T(8,128)(2,1)S(1)} %collective-permute-done.3.refs_4_), channel_id=1, source_target_pairs={{0,2},{1,3},{2,0},{3,1},{4,6},{5,7},{6,4},{7,5},{8,10},{9,11},{10,... | collective-permute-start | bytes 589832 | tf_op jit(solution)/shard_map/ppermute | solution.py:373
  83.5 11.4 %collective-permute-start = (bf16[96,1024]{1,0:T(8,128)(2,1)S(1)}, bf16[96,1024]{1,0:T(8,128)(2,1)S(1)}, u32[]{:S(2)}, u32[]{:S(2)}) collective-permute-start(bf16[96,1024]{1,0:T(8,128)(2,1)S(1)} %copy-done.6), channel_id=1, source_target_pairs={{0,1},{1,0},{2,3},{3,2},{4,5},{5,4},{6,7},{7,6},{8,9},{9,8},{10,11... | collective-permute-start | bytes 589832 | tf_op jit(solution)/shard_map/ppermute | solution.py:373
  83.7 12.1 %collective-permute-start.4 = (bf16[96,1024]{1,0:T(8,128)(2,1)S(1)}, bf16[96,1024]{1,0:T(8,128)(2,1)S(1)}, u32[]{:S(2)}, u32[]{:S(2)}) collective-permute-start(bf16[96,1024]{1,0:T(8,128)(2,1)S(1)} %collective-permute-done.3.refs_4_), channel_id=1, source_target_pairs={{0,1},{1,0},{2,3},{3,2},{4,5},{5,4},{6,7},{7,6},{8,9},{9,8},{10,11... | collective-permute-start | bytes 589832 | tf_op jit(solution)/shard_map/ppermute | solution.py:373
  84.1 11.4 %collective-permute-start.2 = (bf16[96,1024]{1,0:T(8,128)(2,1)S(1)}, bf16[96,1024]{1,0:T(8,128)(2,1)S(1)}, u32[]{:S(2)}, u32[]{:S(2)}) collective-permute-start(bf16[96,1024]{1,0:T(8,128)(2,1)S(1)} %collective-permute-done.1.refs_2_), channel_id=1, source_target_pairs={{0,1},{1,0},{2,3},{3,2},{4,5},{5,4},{6,7},{7,6},{8,9},{9,8},{10,11... | collective-permute-start | bytes 589832 | tf_op jit(solution)/shard_map/ppermute | solution.py:373
  84.2 11.5 %collective-permute-start.6 = (bf16[96,1024]{1,0:T(8,128)(2,1)S(1)}, bf16[96,1024]{1,0:T(8,128)(2,1)S(1)}, u32[]{:S(2)}, u32[]{:S(2)}) collective-permute-start(bf16[96,1024]{1,0:T(8,128)(2,1)S(1)} %collective-permute-done.5.refs_6_), channel_id=1, source_target_pairs={{0,1},{1,0},{2,3},{3,2},{4,5},{5,4},{6,7},{7,6},{8,9},{9,8},{10,11... | collective-permute-start | bytes 589832 | tf_op jit(solution)/shard_map/ppermute | solution.py:373
  84.6 16.0 %collective-permute-start.42 = (bf16[2,192,512]{2,1,0:T(8,128)(2,1)S(1)}, bf16[2,192,512]{2,1,0:T(8,128)(2,1)S(1)}, u32[]{:S(2)}, u32[]{:S(2)}) collective-permute-start(bf16[2,192,512]{2,1,0:T(8,128)(2,1)S(1)} %get-tuple-element.87), channel_id=1, source_target_pairs={{0,1},{1,0},{2,3},{3,2},{4,5},{5,4},{6,7},{7,6},{8,9},{9,8},{10,11... | collective-permute-start | bytes 1179656 | tf_op jit(solution)/shard_map/ppermute | solution.py:373
  101.6 12.0 %collective-permute-start.39 = (bf16[1,192,512]{2,1,0:T(8,128)(2,1)S(1)}, bf16[1,192,512]{2,1,0:T(8,128)(2,1)S(1)}, u32[]{:S(2)}, u32[]{:S(2)}) collective-permute-start(bf16[1,192,512]{2,1,0:T(8,128)(2,1)S(1)} %slice.141), channel_id=1, source_target_pairs={{0,2},{1,3},{2,0},{3,1},{4,6},{5,7},{6,4},{7,5},{8,10},{9,11},{10,... | collective-permute-start | bytes 589832 | tf_op jit(solution)/shard_map/ppermute | solution.py:373
  103.3 13.8 %collective-permute-start.35 = (bf16[1,192,512]{2,1,0:T(8,128)(2,1)S(1)}, bf16[1,192,512]{2,1,0:T(8,128)(2,1)S(1)}, u32[]{:S(2)}, u32[]{:S(2)}) collective-permute-start(bf16[1,192,512]{2,1,0:T(8,128)(2,1)S(1)} %slice.142), channel_id=1, source_target_pairs={{0,2},{1,3},{2,0},{3,1},{4,6},{5,7},{6,4},{7,5},{8,10},{9,11},{10,... | collective-permute-start | bytes 589832 | tf_op jit(solution)/shard_map/ppermute | solution.py:373
  104.0 16.5 %collective-permute-start.32 = (bf16[1,192,512]{2,1,0:T(8,128)(2,1)S(1)}, bf16[1,192,512]{2,1,0:T(8,128)(2,1)S(1)}, u32[]{:S(2)}, u32[]{:S(2)}) collective-permute-start(bf16[1,192,512]{2,1,0:T(8,128)(2,1)S(1)} %slice.143), channel_id=1, source_target_pairs={{0,2},{1,3},{2,0},{3,1},{4,6},{5,7},{6,4},{7,5},{8,10},{9,11},{10,... | collective-permute-start | bytes 589832 | tf_op jit(solution)/shard_map/ppermute | solution.py:373
  108.7 12.9 %collective-permute-start.44 = (bf16[96,512]{1,0:T(8,128)(2,1)S(1)}, bf16[96,512]{1,0:T(8,128)(2,1)S(1)}, u32[]{:S(2)}, u32[]{:S(2)}) collective-permute-start(bf16[96,512]{1,0:T(8,128)(2,1)S(1)} %get-tuple-element.108), channel_id=1, source_target_pairs={{0,24},{4,28},{8,16},{12,20},{16,8},{20,12},{24,0},{28,4},{1,25},{... | collective-permute-start | bytes 294920 | tf_op jit(solution)/shard_map/ppermute | solution.py:373
  111.3 12.4 %collective-permute-start.45 = (bf16[96,512]{1,0:T(8,128)(2,1)S(1)}, bf16[96,512]{1,0:T(8,128)(2,1)S(1)}, u32[]{:S(2)}, u32[]{:S(2)}) collective-permute-start(bf16[96,512]{1,0:T(8,128)(2,1)S(1)} %get-tuple-element.107), channel_id=1, source_target_pairs={{0,28},{4,24},{8,20},{12,16},{16,12},{20,8},{24,4},{28,0},{1,29},{... | collective-permute-start | bytes 294920 | tf_op jit(solution)/shard_map/ppermute | solution.py:373
  113.7 11.5 %collective-permute-start.40 = (bf16[96,512]{1,0:T(8,128)(2,1)S(1)}, bf16[96,512]{1,0:T(8,128)(2,1)S(1)}, u32[]{:S(2)}, u32[]{:S(2)}) collective-permute-start(bf16[96,512]{1,0:T(8,128)(2,1)S(1)} %get-tuple-element.110), channel_id=1, source_target_pairs={{0,16},{4,20},{8,24},{12,28},{16,0},{20,4},{24,8},{28,12},{1,17},{... | collective-permute-start | bytes 294920 | tf_op jit(solution)/shard_map/ppermute | solution.py:373
  133.4 11.6 %collective-permute-start.46 = (bf16[256,512]{1,0:T(8,128)(2,1)}, bf16[256,512]{1,0:T(8,128)(2,1)S(1)}, u32[]{:S(2)}, u32[]{:S(2)}) collective-permute-start(bf16[256,512]{1,0:T(8,128)(2,1)} %shard_map.214.refs_0_), channel_id=1, source_target_pairs={{0,1},{1,0},{2,3},{3,2},{4,5},{5,4},{6,7},{7,6},{8,9},{9,8},{10,11... | collective-permute-start | bytes 786440 | tf_op jit(solution)/shard_map/ppermute | solution.py:373
  147.8 25.3 %collective-permute-start.49 = (bf16[256,256]{1,0:T(8,128)(2,1)}, bf16[256,256]{1,0:T(8,128)(2,1)}, u32[]{:S(2)}, u32[]{:S(2)}) collective-permute-start(bf16[256,256]{1,0:T(8,128)(2,1)} %get-tuple-element.90), channel_id=1, source_target_pairs={{0,4},{4,0},{8,12},{12,8},{16,20},{20,16},{24,28},{28,24},{1,5},{5... | collective-permute-start | bytes 393224 | tf_op jit(solution)/shard_map/ppermute | solution.py:373
  148.0 27.5 %collective-permute-start.50 = (bf16[256,256]{1,0:T(8,128)(2,1)}, bf16[256,256]{1,0:T(8,128)(2,1)}, u32[]{:S(2)}, u32[]{:S(2)}) collective-permute-start(bf16[256,256]{1,0:T(8,128)(2,1)} %get-tuple-element.91), channel_id=1, source_target_pairs={{0,8},{4,12},{8,0},{12,4},{16,24},{20,28},{24,16},{28,20},{1,9},{5... | collective-permute-start | bytes 393224 | tf_op jit(solution)/shard_map/ppermute | solution.py:373
  162.1 33.6 %all-to-all-start = ((f32[8,8,256]{2,1,0:T(8,128)}), f32[8,8,256]{2,1,0:T(8,128)S(1)}, u32[]{:S(2)}, u32[]{:S(2)}) async-start(f32[8,8,256]{2,1,0:T(8,128)} %broadcast_in_dim.18), calls=%async_computation | async-start | bytes 131072 | tf_op jit(solution)/shard_map/all_to_all | solution.py:540
  167.3 35.1 %collective-permute-start.51 = (bf16[256,256]{1,0:T(8,128)(2,1)}, bf16[256,256]{1,0:T(8,128)(2,1)}, u32[]{:S(2)}, u32[]{:S(2)}) collective-permute-start(bf16[256,256]{1,0:T(8,128)(2,1)} %copy-done.65), channel_id=1, source_target_pairs={{0,12},{4,8},{8,4},{12,0},{16,28},{20,24},{24,20},{28,16},{1,13},{... | collective-permute-start | bytes 393224 | tf_op jit(solution)/shard_map/ppermute | solution.py:373
  170.2 32.2 %collective-permute-start.52 = (bf16[256,256]{1,0:T(8,128)(2,1)}, bf16[256,256]{1,0:T(8,128)(2,1)}, u32[]{:S(2)}, u32[]{:S(2)}) collective-permute-start(bf16[256,256]{1,0:T(8,128)(2,1)} %copy-done.64), channel_id=1, source_target_pairs={{0,16},{4,20},{8,24},{12,28},{16,0},{20,4},{24,8},{28,12},{1,17},{... | collective-permute-start | bytes 393224 | tf_op jit(solution)/shard_map/ppermute | solution.py:373
  172.6 29.8 %collective-permute-start.53 = (bf16[256,256]{1,0:T(8,128)(2,1)}, bf16[256,256]{1,0:T(8,128)(2,1)}, u32[]{:S(2)}, u32[]{:S(2)}) collective-permute-start(bf16[256,256]{1,0:T(8,128)(2,1)} %copy-done.63), channel_id=1, source_target_pairs={{0,20},{4,16},{8,28},{12,24},{16,4},{20,0},{24,12},{28,8},{1,21},{... | collective-permute-start | bytes 393224 | tf_op jit(solution)/shard_map/ppermute | solution.py:373
  173.1 29.3 %collective-permute-start.54 = (bf16[256,256]{1,0:T(8,128)(2,1)}, bf16[256,256]{1,0:T(8,128)(2,1)}, u32[]{:S(2)}, u32[]{:S(2)}) collective-permute-start(bf16[256,256]{1,0:T(8,128)(2,1)} %copy-done.62), channel_id=1, source_target_pairs={{0,24},{4,28},{8,16},{12,20},{16,8},{20,12},{24,0},{28,4},{1,25},{... | collective-permute-start | bytes 393224 | tf_op jit(solution)/shard_map/ppermute | solution.py:373
  175.5 26.9 %collective-permute-start.55 = (bf16[256,256]{1,0:T(8,128)(2,1)}, bf16[256,256]{1,0:T(8,128)(2,1)}, u32[]{:S(2)}, u32[]{:S(2)}) collective-permute-start(bf16[256,256]{1,0:T(8,128)(2,1)} %copy-done.61), channel_id=1, source_target_pairs={{0,28},{4,24},{8,20},{12,16},{16,12},{20,8},{24,4},{28,0},{1,29},{... | collective-permute-start | bytes 393224 | tf_op jit(solution)/shard_map/ppermute | solution.py:373
  (91 other events, 1152.6 us)
where the time goes:
time: 206 us; the launch traced here: 205 us
  starting transfers between devices  75.1 us (36%)
  waiting for transfers between devices  50.4 us (24%)
  Pallas kernels  45.7 us (22%)
  local copies, waits for them, and re-layouts  29.2 us (14%)
  other arithmetic  2.72 us (1%)
    ppermute x56, starting transfers between devices, swap(): return lax.ppermute(value, axis, [(i, i ^ bit) for i in range(count)])  70 us
    ppermute x56, waiting for transfers between devices, swap(): return lax.ppermute(value, axis, [(i, i ^ bit) for i in range(count)])  50.4 us
    pallas_call x10, Pallas kernels, call(): pl.pallas_call(kernel, out_shape=tuple(outs), in_specs=specs, out_specs=t...  35.5 us
    unnamed x132, local copies, waits for them, and re-layouts  28.4 us
    pallas_call x2, Pallas kernels, weight_call(): pl.pallas_call(functools.partial(kernel, *sizes), out_shape=tuple(outs),...  9.73 us
    all_to_all x1, starting transfers between devices, scheduled(): lax.all_to_all(jnp.broadcast_to(ends[None], (experts, *ends.shape)), 'sp'...  5.15 us
  transfers between devices with their start and end apart: 57, of which 17 were waited for; matrix products, arithmetic and copies ran while one was open for 1% of the time, Pallas kernels for 19%

commit v1 on v0

--- a/solution.py
+++ b/solution.py
@@ -53,50 +53,46 @@
     for fetch in fetches:
         fetch.start()
     routes_ref, gates_ref, rows_ref, cot_ref = near
-    position_ref, blocks = out_refs[0], out_refs[1:]
+    table_ref, blocks = out_refs[0], out_refs[1:]
     fetches[0].wait()
-    fetches[1].wait()
     top, tokens = routes_ref.shape
-    filler = jnp.zeros((8 - 2 * top % 8, tokens), f32)
-    table = jnp.concatenate([routes_ref[...].astype(f32), gates_ref[...], filler], axis=0).T
     width = rows_ref.shape[1]
-    lanes = max(128, experts)
-    named = lax.broadcasted_iota(jnp.int32, (tokens, lanes), 1)
-    picks = [table[:, k : k + 1].astype(jnp.int32) for k in range(top)]
+    picks = [routes_ref[k : k + 1, :] for k in range(top)]
+    named = lax.broadcasted_iota(jnp.int32, (-(-experts // 16) * 16, tokens), 0)
     onehots = [(pick == named).astype(f32) for pick in picks]
     both = functools.reduce(jnp.add, onehots).astype(bf16)
     before = (
         lax.broadcasted_iota(jnp.int32, (tokens, tokens), 0)
-        > lax.broadcasted_iota(jnp.int32, (tokens, tokens), 1)
+        < lax.broadcasted_iota(jnp.int32, (tokens, tokens), 1)
     ).astype(f32).astype(bf16)
-    earlier = dot(before, both, nn)
-    positions = [
-        jnp.sum(earlier * onehot, axis=1, keepdims=True).astype(jnp.int32) for onehot in onehots
-    ]
+    earlier = dot(both, before, nn)
+    positions = [jnp.sum(earlier * onehot, axis=0, keepdims=True) for onehot in onehots]
+    table_ref[...] = jnp.zeros_like(table_ref)
     for k in range(top):
-        position_ref[:, k : k + 1] = picks[k]
-        position_ref[:, top + k : top + k + 1] = positions[k]
-    for fetch in fetches[2:]:
+        table_ref[k : k + 1, :] = picks[k].astype(f32)
+        table_ref[top + k : top + k + 1, :] = positions[k]
+    for fetch in fetches[1:]:
         fetch.wait()
-    rows = rows_ref[...]
-    cot = cot_ref[...].astype(f32)
-    scaled = [(cot * table[:, top + k : top + k + 1]).astype(bf16) for k in range(top)]
-    slot = lax.broadcasted_iota(jnp.int32, (tokens, capacity), 1)
+    both = jnp.concatenate([rows_ref[...], cot_ref[...]], axis=1)
+    slot = lax.broadcasted_iota(jnp.int32, (capacity, tokens), 0)
     for s in range(experts):
         expert = place_ref[0] ^ s
         selects = [
-            (jnp.where(pick == expert, position, -1) == slot).astype(f32).astype(bf16)
+            (jnp.where(pick == expert, position.astype(jnp.int32), -1) == slot).astype(f32)
             for pick, position in zip(picks, positions)
         ]
-        blocks[s][:, :width] = dot(functools.reduce(jnp.add, selects), rows, tn).astype(bf16)
-        grads = functools.reduce(jnp.add, [dot(sel, sc, tn) for sel, sc in zip(selects, scaled)])
-        blocks[s][:, width:] = grads.astype(bf16)
-
-
-def combine_kernel(experts, place_ref, table_ref, cot_ref, *refs):
+        scales = [sel * gates_ref[k : k + 1, :] for k, sel in enumerate(selects)]
+        scale = jnp.sum(functools.reduce(jnp.add, scales), axis=1, keepdims=True)
+        moved = dot(functools.reduce(jnp.add, selects).astype(bf16), both, nn)
+        blocks[s][:, :width] = moved[:, :width].astype(bf16)
+        blocks[s][:, width:] = (moved[:, width:] * scale).astype(bf16)
+
+
+def combine_kernel(experts, top, place_ref, table_ref, cot_ref, *refs):
     blocks, out_ref = refs[:experts], refs[experts]
-    tokens, top = table_ref.shape[0], table_ref.shape[1] // 2
+    tokens = table_ref.shape[1]
     capacity = blocks[0].shape[0]
+    table = table_ref[...].T.astype(jnp.int32)
     slot = lax.broadcasted_iota(jnp.int32, (tokens, capacity), 1)
     total = cot_ref[...].astype(f32)
     added = jnp.zeros_like(total)
@@ -106,9 +102,7 @@
             jnp.add,
             [
                 (
-                    jnp.where(
-                        table_ref[:, k : k + 1] == expert, table_ref[:, top + k : top + k + 1], -1
-                    )
+                    jnp.where(table[:, k : k + 1] == expert, table[:, top + k : top + k + 1], -1)
                     == slot
                 ).astype(f32)
                 for k in range(top)
@@ -426,7 +420,7 @@
     packed = call(
         functools.partial(pack_kernel, experts, capacity),
         (sp, *inputs),
-        [shape((tokens, 2 * top), jnp.int32)]
+        [shape((-(-2 * top // 8) * 8, tokens), f32)]
         + [shape((capacity, 2 * width), bf16) for _ in range(experts)],
         scratch=[pltpu.VMEM(a.shape, a.dtype) for a in inputs]
         + [pltpu.SemaphoreType.DMA((len(inputs),))],
@@ -509,7 +503,7 @@
     )
 
     (residual_grad,) = call(
-        functools.partial(combine_kernel, experts),
+        functools.partial(combine_kernel, experts, top),
         (sp, table, cotangent, *returned),
         [shape((tokens, width), bf16)],
         flops=2 * tokens * experts * capacity * width,

time: 206 us -> 204 us (level)
  no operation moved by 1% of the time
where the time goes in v1:
time: 204 us; the launch traced here: 203 us
  starting transfers between devices  75 us (37%)
  waiting for transfers between devices  50.4 us (25%)
  Pallas kernels  44.4 us (22%)
  local copies, waits for them, and re-layouts  29.2 us (14%)
  other arithmetic  2.72 us (1%)
    ppermute x56, starting transfers between devices, swap(): return lax.ppermute(value, axis, [(i, i ^ bit) for i in range(count)])  69.9 us
    ppermute x56, waiting for transfers between devices, swap(): return lax.ppermute(value, axis, [(i, i ^ bit) for i in range(count)])  50.4 us
    pallas_call x10, Pallas kernels, call(): pl.pallas_call(kernel, out_shape=tuple(outs), in_specs=specs, out_specs=t...  34.1 us
    unnamed x132, local copies, waits for them, and re-layouts  28.4 us
    pallas_call x2, Pallas kernels, weight_call(): pl.pallas_call(functools.partial(kernel, *sizes), out_shape=tuple(outs),...  9.74 us
    all_to_all x1, starting transfers between devices, scheduled(): lax.all_to_all(jnp.broadcast_to(ends[None], (experts, *ends.shape)), 'sp'...  5.12 us
  transfers between devices with their start and end apart: 57, of which 17 were waited for; matrix products, arithmetic and copies ran while one was open for 1% of the time, Pallas kernels for 19%

profile of v1, /device:TPU:0, one launch (start us, length us, event | category | flops | bytes accessed | tf_op | source)
XLA Modules:
  0.0 203.0 jit_solution(5221655245997053955)
XLA Ops:
  0.6 2.6 %shard_map.207 = (f32[8,256]{1,0:T(8,128)}, bf16[96,1024]{1,0:T(8,128)(2,1)}, bf16[96,1024]{1,0:T(8,128)(2,1)}, bf16[96,1024]{1,0:T(8,128)(2,1)}, bf16[96,1024]{...) custom-call(s32[1]{0:T(128)} %bitcast.1.place_ref.sp_ref, ...), custom_call_target="tpu_custom_call" | custom-call | flops 603979776 | bytes 2109444 | tf_op jit(solution)/shard_map/pallas_call | solution.py:31
  3.2 5.1 %collective-permute-start.23 = (bf16[96,1024]{1,0:T(8,128)(2,1)}, bf16[96,1024]{1,0:T(8,128)(2,1)S(1)}, u32[]{:S(2)}, u32[]{:S(2)}) collective-permute-start(bf16[96,1024]{1,0:T(8,128)(2,1)} %get-tuple-element.63), channel_id=1, source_target_pairs={{0,24},{4,28},{8,16},{12,20},{16,8},{20,12},{24,0},{28,4},{1,25},{... | collective-permute-start | bytes 589832 | tf_op jit(solution)/shard_map/ppermute | solution.py:367
  14.0 17.9 %collective-permute-start.11 = (bf16[96,1024]{1,0:T(8,128)(2,1)}, bf16[96,1024]{1,0:T(8,128)(2,1)S(1)}, u32[]{:S(2)}, u32[]{:S(2)}) collective-permute-start(bf16[96,1024]{1,0:T(8,128)(2,1)} %get-tuple-element.60), channel_id=1, source_target_pairs={{0,12},{4,8},{8,4},{12,0},{16,28},{20,24},{24,20},{28,16},{1,13},{... | collective-permute-start | bytes 589832 | tf_op jit(solution)/shard_map/ppermute | solution.py:367
  32.4 6.5 %collective-permute-done.15.refs_0_.refs_16_ = bf16[96,1024]{1,0:T(8,128)(2,1)S(1)} collective-permute-done((bf16[96,1024]{1,0:T(8,128)(2,1)}, bf16[96,1024]{1,0:T(8,128)(2,1)S(1)}, u32[]{:S(2)}, u32[]{:S(2)}) %collective-permute-start.15) | collective-permute-done | bytes 196640 | tf_op jit(solution)/shard_map/ppermute | solution.py:367
  40.5 2.9 %collective-permute-done.19.refs_4_.refs_20_ = bf16[96,1024]{1,0:T(8,128)(2,1)S(1)} collective-permute-done((bf16[96,1024]{1,0:T(8,128)(2,1)}, bf16[96,1024]{1,0:T(8,128)(2,1)S(1)}, u32[]{:S(2)}, u32[]{:S(2)}) %collective-permute-start.19) | collective-permute-done | bytes 196640 | tf_op jit(solution)/shard_map/ppermute | solution.py:367
  47.4 3.7 %collective-permute-done.25.refs_2_.refs_26_ = bf16[96,1024]{1,0:T(8,128)(2,1)S(1)} collective-permute-done((bf16[96,1024]{1,0:T(8,128)(2,1)S(1)}, bf16[96,1024]{1,0:T(8,128)(2,1)S(1)}, u32[]{:S(2)}, u32[]{:S(2)}) %collective-permute-start.25) | collective-permute-done | bytes 196640 | tf_op jit(solution)/shard_map/ppermute | solution.py:367
  52.6 2.7 %collective-permute-done.29.refs_6_.refs_30_ = bf16[96,1024]{1,0:T(8,128)(2,1)S(1)} collective-permute-done((bf16[96,1024]{1,0:T(8,128)(2,1)S(1)}, bf16[96,1024]{1,0:T(8,128)(2,1)S(1)}, u32[]{:S(2)}, u32[]{:S(2)}) %collective-permute-start.29) | collective-permute-done | bytes 196640 | tf_op jit(solution)/shard_map/ppermute | solution.py:367
  57.4 2.2 %collective-permute-done.17.refs_2_.refs_18_ = bf16[96,1024]{1,0:T(8,128)(2,1)S(1)} collective-permute-done((bf16[96,1024]{1,0:T(8,128)(2,1)S(1)}, bf16[96,1024]{1,0:T(8,128)(2,1)S(1)}, u32[]{:S(2)}, u32[]{:S(2)}) %collective-permute-start.17) | collective-permute-done | bytes 196640 | tf_op jit(solution)/shard_map/ppermute | solution.py:367
  61.1 2.7 %collective-permute-done.21.refs_6_.refs_22_ = bf16[96,1024]{1,0:T(8,128)(2,1)S(1)} collective-permute-done((bf16[96,1024]{1,0:T(8,128)(2,1)S(1)}, bf16[96,1024]{1,0:T(8,128)(2,1)S(1)}, u32[]{:S(2)}, u32[]{:S(2)}) %collective-permute-start.21) | collective-permute-done | bytes 196640 | tf_op jit(solution)/shard_map/ppermute | solution.py:367
  64.4 3.7 %collective-permute-done.9.refs_2_.refs_10_ = bf16[96,1024]{1,0:T(8,128)(2,1)} collective-permute-done((bf16[96,1024]{1,0:T(8,128)(2,1)S(1)}, bf16[96,1024]{1,0:T(8,128)(2,1)}, u32[]{:S(2)}, u32[]{:S(2)}) %collective-permute-start.9) | collective-permute-done | bytes 196640 | tf_op jit(solution)/shard_map/ppermute | solution.py:367
  68.1 2.4 %collective-permute-done.13.refs_6_.refs_14_ = bf16[96,1024]{1,0:T(8,128)(2,1)} collective-permute-done((bf16[96,1024]{1,0:T(8,128)(2,1)S(1)}, bf16[96,1024]{1,0:T(8,128)(2,1)}, u32[]{:S(2)}, u32[]{:S(2)}) %collective-permute-start.13) | collective-permute-done | bytes 196640 | tf_op jit(solution)/shard_map/ppermute | solution.py:367
  75.9 5.5 %shard_map.211 = (bf16[2,192,512]{2,1,0:T(8,128)(2,1)S(1)}, bf16[2,192,512]{2,1,0:T(8,128)(2,1)S(1)}, bf16[192,512]{1,0:T(8,128)(2,1)S(1)}, bf16[192,512]{1,0:T(8,128)(2,1)S(1)}, bf16[192,512]{1,0:T(8,128)(2,1)S(1)}) custom-call(s32[1]{0:T(128)} %ticket.1.place_ref, bf16[96,1024]{1,0:T(8,128)(2,1)S(1)} %collective-permute-done.23.refs_0_.refs_24_, ...), custom_call_target="tpu_custom_call" | custom-call | flops 2013265920 | bytes 9240580 | tf_op jit(solution)/shard_map/pallas_call | solution.py:31
  83.3 4.5 %shard_map.210 = (bf16[2,192,512]{2,1,0:T(8,128)(2,1)S(1)}, bf16[2,192,512]{2,1,0:T(8,128)(2,1)S(1)}, bf16[192,512]{1,0:T(8,128)(2,1)S(1)}, bf16[192,512]{1,0:T(8,128)(2,1)S(1)}, bf16[192,512]{1,0:T(8,128)(2,1)S(1)}) custom-call(s32[1]{0:T(128)} %ticket.1.place_ref, bf16[96,1024]{1,0:T(8,128)(2,1)S(1)} %collective-permute-done.15.refs_0_.refs_16_, ...), custom_call_target="tpu_custom_call" | custom-call | flops 2013265920 | bytes 9240580 | tf_op jit(solution)/shard_map/pallas_call | solution.py:31
  87.9 5.6 %shard_map.209 = (bf16[2,192,512]{2,1,0:T(8,128)(2,1)S(1)}, bf16[2,192,512]{2,1,0:T(8,128)(2,1)S(1)}, bf16[192,512]{1,0:T(8,128)(2,1)S(1)}, bf16[192,512]{1,0:T(8,128)(2,1)S(1)}, bf16[192,512]{1,0:T(8,128)(2,1)S(1)}) custom-call(s32[1]{0:T(128)} %ticket.1.place_ref, bf16[96,1024]{1,0:T(8,128)(2,1)S(1)} %collective-permute-done.7.refs_0_.refs_8_, ...), custom_call_target="tpu_custom_call" | custom-call | flops 2013265920 | bytes 9240580 | tf_op jit(solution)/shard_map/pallas_call | solution.py:31
  94.1 4.7 %shard_map.208 = (bf16[2,192,512]{2,1,0:T(8,128)(2,1)S(1)}, bf16[2,192,512]{2,1,0:T(8,128)(2,1)S(1)}, bf16[192,512]{1,0:T(8,128)(2,1)S(1)}, bf16[192,512]{1,0:T(8,128)(2,1)S(1)}, bf16[192,512]{1,0:T(8,128)(2,1)S(1)}) custom-call(s32[1]{0:T(128)} %ticket.1.place_ref, bf16[96,1024]{1,0:T(8,128)(2,1)S(1)} %copy-done.6, ...), custom_call_target="tpu_custom_call" | custom-call | flops 2013265920 | bytes 9240580 | tf_op jit(solution)/shard_map/pallas_call | solution.py:31
  104.2 3.1 %collective-permute-done.43 = bf16[1,192,512]{2,1,0:T(8,128)(2,1)S(1)} collective-permute-done((bf16[1,192,512]{2,1,0:T(8,128)(2,1)S(1)}, bf16[1,192,512]{2,1,0:T(8,128)(2,1)S(1)}, u32[]{:S(2)}, u32[]{:S(2)}) %collective-permute-start.43) | collective-permute-done | bytes 196640 | tf_op jit(solution)/shard_map/ppermute | solution.py:367
  107.3 2.5 %collective-permute-start.44 = (bf16[96,512]{1,0:T(8,128)(2,1)S(1)}, bf16[96,512]{1,0:T(8,128)(2,1)S(1)}, u32[]{:S(2)}, u32[]{:S(2)}) collective-permute-start(bf16[96,512]{1,0:T(8,128)(2,1)S(1)} %get-tuple-element.108), channel_id=1, source_target_pairs={{0,24},{4,28},{8,16},{12,20},{16,8},{20,12},{24,0},{28,4},{1,25},{... | collective-permute-start | bytes 294920 | tf_op jit(solution)/shard_map/ppermute | solution.py:367
  109.8 2.3 %collective-permute-start.45 = (bf16[96,512]{1,0:T(8,128)(2,1)S(1)}, bf16[96,512]{1,0:T(8,128)(2,1)S(1)}, u32[]{:S(2)}, u32[]{:S(2)}) collective-permute-start(bf16[96,512]{1,0:T(8,128)(2,1)S(1)} %get-tuple-element.107), channel_id=1, source_target_pairs={{0,28},{4,24},{8,20},{12,16},{16,12},{20,8},{24,4},{28,0},{1,29},{... | collective-permute-start | bytes 294920 | tf_op jit(solution)/shard_map/ppermute | solution.py:367
  112.4 3.3 %collective-permute-done.35 = bf16[1,192,512]{2,1,0:T(8,128)(2,1)S(1)} collective-permute-done((bf16[1,192,512]{2,1,0:T(8,128)(2,1)S(1)}, bf16[1,192,512]{2,1,0:T(8,128)(2,1)S(1)}, u32[]{:S(2)}, u32[]{:S(2)}) %collective-permute-start.35) | collective-permute-done | bytes 196640 | tf_op jit(solution)/shard_map/ppermute | solution.py:367
  116.7 2.4 %collective-permute-done.32 = bf16[1,192,512]{2,1,0:T(8,128)(2,1)S(1)} collective-permute-done((bf16[1,192,512]{2,1,0:T(8,128)(2,1)S(1)}, bf16[1,192,512]{2,1,0:T(8,128)(2,1)S(1)}, u32[]{:S(2)}, u32[]{:S(2)}) %collective-permute-start.32) | collective-permute-done | bytes 196640 | tf_op jit(solution)/shard_map/ppermute | solution.py:367
  123.7 2.5 %collective-permute-done.41.refs_5_ = bf16[96,512]{1,0:T(8,128)(2,1)S(1)} collective-permute-done((bf16[96,512]{1,0:T(8,128)(2,1)S(1)}, bf16[96,512]{1,0:T(8,128)(2,1)S(1)}, u32[]{:S(2)}, u32[]{:S(2)}) %collective-permute-start.41) | collective-permute-done | bytes 98336 | tf_op jit(solution)/shard_map/ppermute | solution.py:367
  127.2 2.5 %collective-permute-done.37.refs_3_ = bf16[96,512]{1,0:T(8,128)(2,1)S(1)} collective-permute-done((bf16[96,512]{1,0:T(8,128)(2,1)S(1)}, bf16[96,512]{1,0:T(8,128)(2,1)S(1)}, u32[]{:S(2)}, u32[]{:S(2)}) %collective-permute-start.37) | collective-permute-done | bytes 98336 | tf_op jit(solution)/shard_map/ppermute | solution.py:367
  132.1 7.5 %collective-permute-done.47.refs_2_ = bf16[256,512]{1,0:T(8,128)(2,1)S(1)} collective-permute-done((bf16[256,512]{1,0:T(8,128)(2,1)}, bf16[256,512]{1,0:T(8,128)(2,1)S(1)}, u32[]{:S(2)}, u32[]{:S(2)}) %collective-permute-start.47) | collective-permute-done | bytes 262176 | tf_op jit(solution)/shard_map/ppermute | solution.py:367
  147.3 5.8 %shard_map.212 = (bf16[2048,512]{1,0:T(8,128)(2,1)}, bf16[2048,512]{1,0:T(8,128)(2,1)}) custom-call(s32[1]{0:T(128)} %bitcast.place_ref.tp_ref, bf16[96,1024]{1,0:T(8,128)(2,1)S(1)} %copy-done.6, bf16[96,1024]{1,0:T(8,128)(2,1)S(1)} %collective-permute-done.refs_1_, bf16[96,1024]{1,0:T(8,128)(2,1)S(1)} %collective-permute-done.1.refs_2_, ...), custom_call_target="tpu_custom_call" | custom-call | flops 3221225472 | bytes 5242880 | tf_op jit(solution)/shard_map/pallas_call | solution.py:475
  153.1 5.2 %shard_map.217 = (f32[256,256]{1,0:T(8,128)}, f32[2,256,256]{2,1,0:T(8,128)S(1)}, f32[2,256,256]{2,1,0:T(8,128)S(1)}, f32[8,256]{1,0:T(8,128)S(1)}) custom-call(s32[1]{0:T(128)} %bitcast.place_ref.tp_ref, bf16[256,2048]{1,0:T(8,128)(2,1)S(1)} %copy-done.5, f32[256,256]{1,0:T(8,128)S(1)} %get-tuple-element.97.gelu_ref, ...), custom_call_target="tpu_custom_call" | custom-call | flops 268435456 | bytes 4464644 | tf_op jit(solution)/shard_map/pallas_call | solution.py:31
  160.6 5.1 %all-to-all-start = ((f32[8,8,256]{2,1,0:T(8,128)}), f32[8,8,256]{2,1,0:T(8,128)S(1)}, u32[]{:S(2)}, u32[]{:S(2)}) async-start(f32[8,8,256]{2,1,0:T(8,128)} %broadcast_in_dim.18), calls=%async_computation | async-start | bytes 131072 | tf_op jit(solution)/shard_map/all_to_all | solution.py:534
  165.7 2.9 %collective-permute-start.51 = (bf16[256,256]{1,0:T(8,128)(2,1)}, bf16[256,256]{1,0:T(8,128)(2,1)}, u32[]{:S(2)}, u32[]{:S(2)}) collective-permute-start(bf16[256,256]{1,0:T(8,128)(2,1)} %copy-done.65), channel_id=1, source_target_pairs={{0,12},{4,8},{8,4},{12,0},{16,28},{20,24},{24,20},{28,16},{1,13},{... | collective-permute-start | bytes 393224 | tf_op jit(solution)/shard_map/ppermute | solution.py:367
  168.7 2.4 %collective-permute-start.52 = (bf16[256,256]{1,0:T(8,128)(2,1)}, bf16[256,256]{1,0:T(8,128)(2,1)}, u32[]{:S(2)}, u32[]{:S(2)}) collective-permute-start(bf16[256,256]{1,0:T(8,128)(2,1)} %copy-done.64), channel_id=1, source_target_pairs={{0,16},{4,20},{8,24},{12,28},{16,0},{20,4},{24,8},{28,12},{1,17},{... | collective-permute-start | bytes 393224 | tf_op jit(solution)/shard_map/ppermute | solution.py:367
  171.6 2.4 %collective-permute-start.54 = (bf16[256,256]{1,0:T(8,128)(2,1)}, bf16[256,256]{1,0:T(8,128)(2,1)}, u32[]{:S(2)}, u32[]{:S(2)}) collective-permute-start(bf16[256,256]{1,0:T(8,128)(2,1)} %copy-done.62), channel_id=1, source_target_pairs={{0,24},{4,28},{8,16},{12,20},{16,8},{20,12},{24,0},{28,4},{1,25},{... | collective-permute-start | bytes 393224 | tf_op jit(solution)/shard_map/ppermute | solution.py:367
  174.0 2.4 %collective-permute-start.55 = (bf16[256,256]{1,0:T(8,128)(2,1)}, bf16[256,256]{1,0:T(8,128)(2,1)}, u32[]{:S(2)}, u32[]{:S(2)}) collective-permute-start(bf16[256,256]{1,0:T(8,128)(2,1)} %copy-done.61), channel_id=1, source_target_pairs={{0,28},{4,24},{8,20},{12,16},{16,12},{20,8},{24,4},{28,0},{1,29},{... | collective-permute-start | bytes 393224 | tf_op jit(solution)/shard_map/ppermute | solution.py:367
  190.2 4.0 %shard_map.213 = bf16[512,2048]{1,0:T(8,128)(2,1)} custom-call(s32[1]{0:T(128)} %bitcast.place_ref.tp_ref, bf16[96,1024]{1,0:T(8,128)(2,1)S(1)} %copy-done.6, bf16[96,1024]{1,0:T(8,128)(2,1)S(1)} %copy-done.24, bf16[96,1024]{1,0:T(8,128)(2,1)S(1)} %collective-permute-done.1.refs_2_, bf16[96,1024]{1,0:T(8,128)(2,1)S(1)} %copy-done.28, ...), custom_call_target="tpu_custom_call" | custom-call | flops 1610612736 | bytes 5242880 | tf_op jit(solution)/shard_map/pallas_call | solution.py:475
  200.9 2.1 %convert_add_fusion.4 = f32[256,256]{1,0:T(8,128)} fusion(bf16[256,256]{1,0:T(8,128)(2,1)} %collective-permute-done.55, bf16[256,256]{1,0:T(8,128)(2,1)} %collective-permute-done.54, bf16[256,256]{1,0:T(8,128)(2,1)} %collective-permute-done.53, bf16[256,256]{1,0:T(8,128)(2,1)} %collective-permute-done.52, bf16[256,256]{1,0:T(8,128)(2,1)} %collective-permute-done.51, ...), kind=kLoop, calls=%fused_computation.16 | loop fusion | flops 983040 | bytes 1310720 | tf_op jit(solution)/shard_map/add | solution.py:544
  (245 shorter events, 70.6 us)
Async XLA Ops:
  3.2 10.8 %collective-permute-start.23 = (bf16[96,1024]{1,0:T(8,128)(2,1)}, bf16[96,1024]{1,0:T(8,128)(2,1)S(1)}, u32[]{:S(2)}, u32[]{:S(2)}) collective-permute-start(bf16[96,1024]{1,0:T(8,128)(2,1)} %get-tuple-element.63), channel_id=1, source_target_pairs={{0,24},{4,28},{8,16},{12,20},{16,8},{20,12},{24,0},{28,4},{1,25},{... | collective-permute-start | bytes 589832 | tf_op jit(solution)/shard_map/ppermute | solution.py:367
  8.4 23.6 %collective-permute-start.27 = (bf16[96,1024]{1,0:T(8,128)(2,1)}, bf16[96,1024]{1,0:T(8,128)(2,1)S(1)}, u32[]{:S(2)}, u32[]{:S(2)}) collective-permute-start(bf16[96,1024]{1,0:T(8,128)(2,1)} %get-tuple-element.64), channel_id=1, source_target_pairs={{0,28},{4,24},{8,20},{12,16},{16,12},{20,8},{24,4},{28,0},{1,29},{... | collective-permute-start | bytes 589832 | tf_op jit(solution)/shard_map/ppermute | solution.py:367
  9.5 29.4 %collective-permute-start.15 = (bf16[96,1024]{1,0:T(8,128)(2,1)}, bf16[96,1024]{1,0:T(8,128)(2,1)S(1)}, u32[]{:S(2)}, u32[]{:S(2)}) collective-permute-start(bf16[96,1024]{1,0:T(8,128)(2,1)} %get-tuple-element.61), channel_id=1, source_target_pairs={{0,16},{4,20},{8,24},{12,28},{16,0},{20,4},{24,8},{28,12},{1,17},{... | collective-permute-start | bytes 589832 | tf_op jit(solution)/shard_map/ppermute | solution.py:367
  10.3 33.0 %collective-permute-start.19 = (bf16[96,1024]{1,0:T(8,128)(2,1)}, bf16[96,1024]{1,0:T(8,128)(2,1)S(1)}, u32[]{:S(2)}, u32[]{:S(2)}) collective-permute-start(bf16[96,1024]{1,0:T(8,128)(2,1)} %get-tuple-element.62), channel_id=1, source_target_pairs={{0,20},{4,16},{8,28},{12,24},{16,4},{20,0},{24,12},{28,8},{1,21},{... | collective-permute-start | bytes 589832 | tf_op jit(solution)/shard_map/ppermute | solution.py:367
  12.3 32.6 %collective-permute-start.7 = (bf16[96,1024]{1,0:T(8,128)(2,1)}, bf16[96,1024]{1,0:T(8,128)(2,1)S(1)}, u32[]{:S(2)}, u32[]{:S(2)}) collective-permute-start(bf16[96,1024]{1,0:T(8,128)(2,1)} %get-tuple-element.59), channel_id=1, source_target_pairs={{0,8},{4,12},{8,0},{12,4},{16,24},{20,28},{24,16},{28,20},{1,9},{5... | collective-permute-start | bytes 589832 | tf_op jit(solution)/shard_map/ppermute | solution.py:367
  14.0 31.4 %collective-permute-start.11 = (bf16[96,1024]{1,0:T(8,128)(2,1)}, bf16[96,1024]{1,0:T(8,128)(2,1)S(1)}, u32[]{:S(2)}, u32[]{:S(2)}) collective-permute-start(bf16[96,1024]{1,0:T(8,128)(2,1)} %get-tuple-element.60), channel_id=1, source_target_pairs={{0,12},{4,8},{8,4},{12,0},{16,28},{20,24},{24,20},{28,16},{1,13},{... | collective-permute-start | bytes 589832 | tf_op jit(solution)/shard_map/ppermute | solution.py:367
  31.9 13.5 %collective-permute-start.3 = (bf16[96,1024]{1,0:T(8,128)(2,1)}, bf16[96,1024]{1,0:T(8,128)(2,1)S(1)}, u32[]{:S(2)}, u32[]{:S(2)}) collective-permute-start(bf16[96,1024]{1,0:T(8,128)(2,1)} %get-tuple-element.58), channel_id=1, source_target_pairs={{0,4},{4,0},{8,12},{12,8},{16,20},{20,16},{24,28},{28,24},{1,5},{5... | collective-permute-start | bytes 589832 | tf_op jit(solution)/shard_map/ppermute | solution.py:367
  45.9 13.6 %collective-permute-start.17 = (bf16[96,1024]{1,0:T(8,128)(2,1)S(1)}, bf16[96,1024]{1,0:T(8,128)(2,1)S(1)}, u32[]{:S(2)}, u32[]{:S(2)}) collective-permute-start(bf16[96,1024]{1,0:T(8,128)(2,1)S(1)} %collective-permute-done.15.refs_0_.refs_16_), channel_id=1, source_target_pairs={{0,2},{1,3},{2,0},{3,1},{4,6},{5,7},{6,4},{7,5},{8,10},{9,11},{10,... | collective-permute-start | bytes 589832 | tf_op jit(solution)/shard_map/ppermute | solution.py:367
  51.1 12.6 %collective-permute-start.21 = (bf16[96,1024]{1,0:T(8,128)(2,1)S(1)}, bf16[96,1024]{1,0:T(8,128)(2,1)S(1)}, u32[]{:S(2)}, u32[]{:S(2)}) collective-permute-start(bf16[96,1024]{1,0:T(8,128)(2,1)S(1)} %collective-permute-done.19.refs_4_.refs_20_), channel_id=1, source_target_pairs={{0,2},{1,3},{2,0},{3,1},{4,6},{5,7},{6,4},{7,5},{8,10},{9,11},{10,... | collective-permute-start | bytes 589832 | tf_op jit(solution)/shard_map/ppermute | solution.py:367
  55.8 12.2 %collective-permute-start.9 = (bf16[96,1024]{1,0:T(8,128)(2,1)S(1)}, bf16[96,1024]{1,0:T(8,128)(2,1)}, u32[]{:S(2)}, u32[]{:S(2)}) collective-permute-start(bf16[96,1024]{1,0:T(8,128)(2,1)S(1)} %collective-permute-done.7.refs_0_.refs_8_), channel_id=1, source_target_pairs={{0,2},{1,3},{2,0},{3,1},{4,6},{5,7},{6,4},{7,5},{8,10},{9,11},{10,... | collective-permute-start | bytes 589832 | tf_op jit(solution)/shard_map/ppermute | solution.py:367
  59.5 10.9 %collective-permute-start.13 = (bf16[96,1024]{1,0:T(8,128)(2,1)S(1)}, bf16[96,1024]{1,0:T(8,128)(2,1)}, u32[]{:S(2)}, u32[]{:S(2)}) collective-permute-start(bf16[96,1024]{1,0:T(8,128)(2,1)S(1)} %collective-permute-done.11.refs_4_.refs_12_), channel_id=1, source_target_pairs={{0,2},{1,3},{2,0},{3,1},{4,6},{5,7},{6,4},{7,5},{8,10},{9,11},{10,... | collective-permute-start | bytes 589832 | tf_op jit(solution)/shard_map/ppermute | solution.py:367
  70.4 11.6 %collective-permute-start.5 = (bf16[96,1024]{1,0:T(8,128)(2,1)S(1)}, bf16[96,1024]{1,0:T(8,128)(2,1)S(1)}, u32[]{:S(2)}, u32[]{:S(2)}) collective-permute-start(bf16[96,1024]{1,0:T(8,128)(2,1)S(1)} %collective-permute-done.3.refs_4_), channel_id=1, source_target_pairs={{0,2},{1,3},{2,0},{3,1},{4,6},{5,7},{6,4},{7,5},{8,10},{9,11},{10,... | collective-permute-start | bytes 589832 | tf_op jit(solution)/shard_map/ppermute | solution.py:367
  82.1 11.4 %collective-permute-start = (bf16[96,1024]{1,0:T(8,128)(2,1)S(1)}, bf16[96,1024]{1,0:T(8,128)(2,1)S(1)}, u32[]{:S(2)}, u32[]{:S(2)}) collective-permute-start(bf16[96,1024]{1,0:T(8,128)(2,1)S(1)} %copy-done.6), channel_id=1, source_target_pairs={{0,1},{1,0},{2,3},{3,2},{4,5},{5,4},{6,7},{7,6},{8,9},{9,8},{10,11... | collective-permute-start | bytes 589832 | tf_op jit(solution)/shard_map/ppermute | solution.py:367
  82.2 11.9 %collective-permute-start.4 = (bf16[96,1024]{1,0:T(8,128)(2,1)S(1)}, bf16[96,1024]{1,0:T(8,128)(2,1)S(1)}, u32[]{:S(2)}, u32[]{:S(2)}) collective-permute-start(bf16[96,1024]{1,0:T(8,128)(2,1)S(1)} %collective-permute-done.3.refs_4_), channel_id=1, source_target_pairs={{0,1},{1,0},{2,3},{3,2},{4,5},{5,4},{6,7},{7,6},{8,9},{9,8},{10,11... | collective-permute-start | bytes 589832 | tf_op jit(solution)/shard_map/ppermute | solution.py:367
  82.7 11.2 %collective-permute-start.2 = (bf16[96,1024]{1,0:T(8,128)(2,1)S(1)}, bf16[96,1024]{1,0:T(8,128)(2,1)S(1)}, u32[]{:S(2)}, u32[]{:S(2)}) collective-permute-start(bf16[96,1024]{1,0:T(8,128)(2,1)S(1)} %collective-permute-done.1.refs_2_), channel_id=1, source_target_pairs={{0,1},{1,0},{2,3},{3,2},{4,5},{5,4},{6,7},{7,6},{8,9},{9,8},{10,11... | collective-permute-start | bytes 589832 | tf_op jit(solution)/shard_map/ppermute | solution.py:367
  82.8 11.4 %collective-permute-start.6 = (bf16[96,1024]{1,0:T(8,128)(2,1)S(1)}, bf16[96,1024]{1,0:T(8,128)(2,1)S(1)}, u32[]{:S(2)}, u32[]{:S(2)}) collective-permute-start(bf16[96,1024]{1,0:T(8,128)(2,1)S(1)} %collective-permute-done.5.refs_6_), channel_id=1, source_target_pairs={{0,1},{1,0},{2,3},{3,2},{4,5},{5,4},{6,7},{7,6},{8,9},{9,8},{10,11... | collective-permute-start | bytes 589832 | tf_op jit(solution)/shard_map/ppermute | solution.py:367
  83.2 16.0 %collective-permute-start.42 = (bf16[2,192,512]{2,1,0:T(8,128)(2,1)S(1)}, bf16[2,192,512]{2,1,0:T(8,128)(2,1)S(1)}, u32[]{:S(2)}, u32[]{:S(2)}) collective-permute-start(bf16[2,192,512]{2,1,0:T(8,128)(2,1)S(1)} %get-tuple-element.87), channel_id=1, source_target_pairs={{0,1},{1,0},{2,3},{3,2},{4,5},{5,4},{6,7},{7,6},{8,9},{9,8},{10,11... | collective-permute-start | bytes 1179656 | tf_op jit(solution)/shard_map/ppermute | solution.py:367
  100.1 12.0 %collective-permute-start.39 = (bf16[1,192,512]{2,1,0:T(8,128)(2,1)S(1)}, bf16[1,192,512]{2,1,0:T(8,128)(2,1)S(1)}, u32[]{:S(2)}, u32[]{:S(2)}) collective-permute-start(bf16[1,192,512]{2,1,0:T(8,128)(2,1)S(1)} %slice.141), channel_id=1, source_target_pairs={{0,2},{1,3},{2,0},{3,1},{4,6},{5,7},{6,4},{7,5},{8,10},{9,11},{10,... | collective-permute-start | bytes 589832 | tf_op jit(solution)/shard_map/ppermute | solution.py:367
  101.8 13.8 %collective-permute-start.35 = (bf16[1,192,512]{2,1,0:T(8,128)(2,1)S(1)}, bf16[1,192,512]{2,1,0:T(8,128)(2,1)S(1)}, u32[]{:S(2)}, u32[]{:S(2)}) collective-permute-start(bf16[1,192,512]{2,1,0:T(8,128)(2,1)S(1)} %slice.142), channel_id=1, source_target_pairs={{0,2},{1,3},{2,0},{3,1},{4,6},{5,7},{6,4},{7,5},{8,10},{9,11},{10,... | collective-permute-start | bytes 589832 | tf_op jit(solution)/shard_map/ppermute | solution.py:367
  102.6 16.5 %collective-permute-start.32 = (bf16[1,192,512]{2,1,0:T(8,128)(2,1)S(1)}, bf16[1,192,512]{2,1,0:T(8,128)(2,1)S(1)}, u32[]{:S(2)}, u32[]{:S(2)}) collective-permute-start(bf16[1,192,512]{2,1,0:T(8,128)(2,1)S(1)} %slice.143), channel_id=1, source_target_pairs={{0,2},{1,3},{2,0},{3,1},{4,6},{5,7},{6,4},{7,5},{8,10},{9,11},{10,... | collective-permute-start | bytes 589832 | tf_op jit(solution)/shard_map/ppermute | solution.py:367
  107.3 12.8 %collective-permute-start.44 = (bf16[96,512]{1,0:T(8,128)(2,1)S(1)}, bf16[96,512]{1,0:T(8,128)(2,1)S(1)}, u32[]{:S(2)}, u32[]{:S(2)}) collective-permute-start(bf16[96,512]{1,0:T(8,128)(2,1)S(1)} %get-tuple-element.108), channel_id=1, source_target_pairs={{0,24},{4,28},{8,16},{12,20},{16,8},{20,12},{24,0},{28,4},{1,25},{... | collective-permute-start | bytes 294920 | tf_op jit(solution)/shard_map/ppermute | solution.py:367
  109.8 12.4 %collective-permute-start.45 = (bf16[96,512]{1,0:T(8,128)(2,1)S(1)}, bf16[96,512]{1,0:T(8,128)(2,1)S(1)}, u32[]{:S(2)}, u32[]{:S(2)}) collective-permute-start(bf16[96,512]{1,0:T(8,128)(2,1)S(1)} %get-tuple-element.107), channel_id=1, source_target_pairs={{0,28},{4,24},{8,20},{12,16},{16,12},{20,8},{24,4},{28,0},{1,29},{... | collective-permute-start | bytes 294920 | tf_op jit(solution)/shard_map/ppermute | solution.py:367
  112.3 11.4 %collective-permute-start.40 = (bf16[96,512]{1,0:T(8,128)(2,1)S(1)}, bf16[96,512]{1,0:T(8,128)(2,1)S(1)}, u32[]{:S(2)}, u32[]{:S(2)}) collective-permute-start(bf16[96,512]{1,0:T(8,128)(2,1)S(1)} %get-tuple-element.110), channel_id=1, source_target_pairs={{0,16},{4,20},{8,24},{12,28},{16,0},{20,4},{24,8},{28,12},{1,17},{... | collective-permute-start | bytes 294920 | tf_op jit(solution)/shard_map/ppermute | solution.py:367
  132.1 11.6 %collective-permute-start.46 = (bf16[256,512]{1,0:T(8,128)(2,1)}, bf16[256,512]{1,0:T(8,128)(2,1)S(1)}, u32[]{:S(2)}, u32[]{:S(2)}) collective-permute-start(bf16[256,512]{1,0:T(8,128)(2,1)} %shard_map.214.refs_0_), channel_id=1, source_target_pairs={{0,1},{1,0},{2,3},{3,2},{4,5},{5,4},{6,7},{7,6},{8,9},{9,8},{10,11... | collective-permute-start | bytes 786440 | tf_op jit(solution)/shard_map/ppermute | solution.py:367
  146.5 25.1 %collective-permute-start.49 = (bf16[256,256]{1,0:T(8,128)(2,1)}, bf16[256,256]{1,0:T(8,128)(2,1)}, u32[]{:S(2)}, u32[]{:S(2)}) collective-permute-start(bf16[256,256]{1,0:T(8,128)(2,1)} %get-tuple-element.90), channel_id=1, source_target_pairs={{0,4},{4,0},{8,12},{12,8},{16,20},{20,16},{24,28},{28,24},{1,5},{5... | collective-permute-start | bytes 393224 | tf_op jit(solution)/shard_map/ppermute | solution.py:367
  146.7 27.2 %collective-permute-start.50 = (bf16[256,256]{1,0:T(8,128)(2,1)}, bf16[256,256]{1,0:T(8,128)(2,1)}, u32[]{:S(2)}, u32[]{:S(2)}) collective-permute-start(bf16[256,256]{1,0:T(8,128)(2,1)} %get-tuple-element.91), channel_id=1, source_target_pairs={{0,8},{4,12},{8,0},{12,4},{16,24},{20,28},{24,16},{28,20},{1,9},{5... | collective-permute-start | bytes 393224 | tf_op jit(solution)/shard_map/ppermute | solution.py:367
  160.6 33.6 %all-to-all-start = ((f32[8,8,256]{2,1,0:T(8,128)}), f32[8,8,256]{2,1,0:T(8,128)S(1)}, u32[]{:S(2)}, u32[]{:S(2)}) async-start(f32[8,8,256]{2,1,0:T(8,128)} %broadcast_in_dim.18), calls=%async_computation | async-start | bytes 131072 | tf_op jit(solution)/shard_map/all_to_all | solution.py:534
  165.7 35.1 %collective-permute-start.51 = (bf16[256,256]{1,0:T(8,128)(2,1)}, bf16[256,256]{1,0:T(8,128)(2,1)}, u32[]{:S(2)}, u32[]{:S(2)}) collective-permute-start(bf16[256,256]{1,0:T(8,128)(2,1)} %copy-done.65), channel_id=1, source_target_pairs={{0,12},{4,8},{8,4},{12,0},{16,28},{20,24},{24,20},{28,16},{1,13},{... | collective-permute-start | bytes 393224 | tf_op jit(solution)/shard_map/ppermute | solution.py:367
  168.7 32.2 %collective-permute-start.52 = (bf16[256,256]{1,0:T(8,128)(2,1)}, bf16[256,256]{1,0:T(8,128)(2,1)}, u32[]{:S(2)}, u32[]{:S(2)}) collective-permute-start(bf16[256,256]{1,0:T(8,128)(2,1)} %copy-done.64), channel_id=1, source_target_pairs={{0,16},{4,20},{8,24},{12,28},{16,0},{20,4},{24,8},{28,12},{1,17},{... | collective-permute-start | bytes 393224 | tf_op jit(solution)/shard_map/ppermute | solution.py:367
  171.0 29.8 %collective-permute-start.53 = (bf16[256,256]{1,0:T(8,128)(2,1)}, bf16[256,256]{1,0:T(8,128)(2,1)}, u32[]{:S(2)}, u32[]{:S(2)}) collective-permute-start(bf16[256,256]{1,0:T(8,128)(2,1)} %copy-done.63), channel_id=1, source_target_pairs={{0,20},{4,16},{8,28},{12,24},{16,4},{20,0},{24,12},{28,8},{1,21},{... | collective-permute-start | bytes 393224 | tf_op jit(solution)/shard_map/ppermute | solution.py:367
  171.6 29.3 %collective-permute-start.54 = (bf16[256,256]{1,0:T(8,128)(2,1)}, bf16[256,256]{1,0:T(8,128)(2,1)}, u32[]{:S(2)}, u32[]{:S(2)}) collective-permute-start(bf16[256,256]{1,0:T(8,128)(2,1)} %copy-done.62), channel_id=1, source_target_pairs={{0,24},{4,28},{8,16},{12,20},{16,8},{20,12},{24,0},{28,4},{1,25},{... | collective-permute-start | bytes 393224 | tf_op jit(solution)/shard_map/ppermute | solution.py:367
  174.0 26.9 %collective-permute-start.55 = (bf16[256,256]{1,0:T(8,128)(2,1)}, bf16[256,256]{1,0:T(8,128)(2,1)}, u32[]{:S(2)}, u32[]{:S(2)}) collective-permute-start(bf16[256,256]{1,0:T(8,128)(2,1)} %copy-done.61), channel_id=1, source_target_pairs={{0,28},{4,24},{8,20},{12,16},{16,12},{20,8},{24,4},{28,0},{1,29},{... | collective-permute-start | bytes 393224 | tf_op jit(solution)/shard_map/ppermute | solution.py:367
  (91 other events, 1155.6 us)
